TPU v7x, 512 devices: a whole 4x8x8 slice. The times are simulated.
512 devices in a mesh: ep: 32 (over z, x), tp: 16 (over y, core).
Axes of the slice: x: 4, y: 8, z: 8, core: 2. Of those that a mesh axis runs over, the one named last changes fastest.
Arguments:
- conv_value: bfloat16 [16384, 2048], P('ep', 'tp'), may hold values from -6 to 6
- conv_gate: bfloat16 [16384, 2048], P('ep', 'tp'), may hold values from -9 to 9
- conv_taps: float32 [31, 2048], P(None, 'tp'), may hold values from -14 to 14
- norm_gain: float32 [2048], P('tp'), may hold values from 0.1 to 1.9
- norm_shift: float32 [2048], P('tp'), may hold values from -3 to 3
- conv_out_weight: bfloat16 [2048, 2048], P(None, 'tp'), may hold values from -0.125 to 0.125
- moe_input: bfloat16 [4096, 2048], P('ep'), may hold values from -6 to 6
- moe_gain: float32 [2048], replicated, may hold values from 0.1 to 1.9
- routes: int32 [4096, 4], P('ep'), may hold values from 0 to 31, all different within a row; in each aligned block of 128 rows (0 to 127, 128 to 255, ...) at most 32 rows name the same one
- route_weights: float32 [4096, 4], P('ep'), may hold values from 0.25 to 1
- expert_gate: bfloat16 [32, 2048, 4096], P('ep', None, 'tp'), may hold values from -0.125 to 0.125
- expert_up: bfloat16 [32, 2048, 4096], P('ep', None, 'tp'), may hold values from -0.125 to 0.125
- expert_down: bfloat16 [32, 4096, 2048], P('ep', None, 'tp'), may hold values from -0.09375 to 0.09375
- shared_gate: bfloat16 [2048, 512], P(None, 'tp'), may hold values from -0.125 to 0.125
- shared_up: bfloat16 [2048, 512], P(None, 'tp'), may hold values from -0.125 to 0.125
- shared_down: bfloat16 [512, 2048], P(None, 'tp'), may hold values from -0.25 to 0.25
Outputs:
- conv_result: bfloat16 [16384, 2048], P('ep', 'tp')
- moe_result: bfloat16 [4096, 2048], P('ep', 'tp')
Inputs may be any that keep to these rules, and one draw needn't show every extreme that they name: `routes`: in the rows of one device (aligned blocks of 128 rows) no expert is named by more than 32 rows, a bound that some block reaches; each row names 4 different experts.
All inputs are finite; a program needn't handle non-finite values.
Results may differ from a plain program's by a relative error of at most 0.0068.
Values may be sent and summed in bfloat16 or wider, within the bound.
A program may use at most 64 MiB of HBM per device.

v0:
```python
import jax
import jax.numpy as jnp
from jax import lax
from jax.sharding import Mesh
from jax.sharding import PartitionSpec as P

EP = ("ep_0", "ep_1")


def from_behind(value, axis, steps):
    count = lax.axis_size(axis)
    initial, last = (max(0, -steps), min(count, count - steps))
    return lax.ppermute(value, axis, [(source, source + steps) for source in range(initial, last)])


def cut_along(array, dim, peers):
    before, after = (array.shape[:dim], array.shape[dim + 1 :])
    return jnp.moveaxis(array.reshape(*before, peers, -1, *after), dim, 0)


def joined_along(parts, dim):
    lengths = list(parts.shape[1:])
    lengths[dim] *= parts.shape[0]
    return jnp.moveaxis(parts, 0, dim).reshape(lengths)


def exchange_in_order(parts, axes, turns):
    lengths = [lax.axis_size(a) for a in axes]
    parts = parts.reshape(*lengths, *parts.shape[1:])
    for k in turns:
        parts = lax.all_to_all(parts, axes[k], split_axis=k, concat_axis=k, tiled=True)
    return parts.reshape(-1, *parts.shape[len(axes) :])


def stepwise_exchange(array, axes, turns, split_dim, concat_dim):
    parts = cut_along(array, split_dim, lax.axis_size(axes))
    return joined_along(exchange_in_order(parts, axes, turns), concat_dim)


def body(
    conv_value,
    conv_gate,
    conv_taps,
    norm_gain,
    norm_shift,
    conv_out_weight,
    moe_input,
    moe_gain,
    routes,
    route_weights,
    expert_gate,
    expert_up,
    expert_down,
    shared_gate,
    shared_up,
    shared_down,
):
    tap_count = conv_taps.shape[0]
    rows_a = conv_value.shape[0]
    glu_rows = (
        conv_value.astype(jnp.float32) * jax.nn.sigmoid(conv_gate.astype(jnp.float32))
    ).astype(jnp.bfloat16)
    before = from_behind(glu_rows[rows_a - (tap_count - 1) :], EP, 1)
    padded = jnp.concatenate([before, glu_rows], axis=0)
    filtered = jnp.zeros(glu_rows.shape, jnp.float32)
    for offset in range(tap_count):
        filtered = filtered + conv_taps[offset] * padded[offset : offset + rows_a].astype(
            jnp.float32
        )
    row_total, squares = lax.psum(
        (jnp.sum(filtered, axis=1), jnp.sum(filtered * filtered, axis=1)), "tp"
    )
    channels = conv_out_weight.shape[0]
    row_mean = row_total / channels
    row_square = squares / channels
    scaled = (filtered - row_mean[:, None]) * lax.rsqrt(row_square - row_mean * row_mean + 1e-05)[
        :, None
    ]
    conv_hidden = jax.nn.silu(scaled * norm_gain + norm_shift).astype(jnp.bfloat16)
    conv_sum = jnp.dot(
        lax.all_gather(conv_hidden, "tp", axis=1, tiled=True),
        conv_out_weight,
        preferred_element_type=jnp.float32,
    )
    conv_result = conv_sum.astype(jnp.bfloat16)
    inputs = moe_input.astype(jnp.float32)
    normed = (
        inputs * lax.rsqrt(jnp.mean(inputs * inputs, axis=1, keepdims=True) + 1e-06) * moe_gain
    ).astype(jnp.bfloat16)
    rows_b, per_row = routes.shape
    model_width = normed.shape[1]
    groups = lax.axis_size(EP)
    capacity = 2 * rows_b * per_row // groups
    flat_expert = routes.reshape(-1)
    owner_row = jnp.arange(rows_b * per_row, dtype=jnp.int32) // per_row
    expert_hits = (flat_expert[:, None] == jnp.arange(groups, dtype=jnp.int32)[None, :]).astype(
        jnp.int32
    )
    slot_rank = jnp.sum((jnp.cumsum(expert_hits, axis=0) - expert_hits) * expert_hits, axis=1)
    slot_index = flat_expert * capacity + slot_rank
    outgoing = (
        jnp.zeros((groups * capacity, model_width), jnp.bfloat16)
        .at[slot_index]
        .set(normed[owner_row])
    )
    outgoing = outgoing.reshape(groups, capacity, model_width)
    slot_share = capacity // lax.axis_size("tp")
    own_slots = lax.dynamic_slice_in_dim(outgoing, lax.axis_index("tp") * slot_share, slot_share, 1)
    partial_rows = lax.all_to_all(own_slots, EP, split_axis=0, concat_axis=0, tiled=True)
    arrived = lax.all_gather(partial_rows, "tp", axis=1, tiled=True)
    arrived_rows = arrived.reshape(groups * capacity, model_width)
    gate_value = jnp.dot(arrived_rows, expert_gate[0], preferred_element_type=jnp.float32)
    upward = jnp.dot(arrived_rows, expert_up[0], preferred_element_type=jnp.float32)
    expert_hidden = (jax.nn.silu(gate_value) * upward).astype(jnp.bfloat16)
    shared_hidden = (
        jax.nn.silu(jnp.dot(normed, shared_gate, preferred_element_type=jnp.float32))
        * jnp.dot(normed, shared_up, preferred_element_type=jnp.float32)
    ).astype(jnp.bfloat16)
    columns = expert_down.shape[2]
    routed_rows = expert_down[0]
    routed_sum = jnp.dot(
        lax.all_gather(expert_hidden, "tp", axis=1, tiled=True),
        routed_rows,
        preferred_element_type=jnp.float32,
    )
    shared_sum = jnp.dot(
        lax.all_gather(shared_hidden, "tp", axis=1, tiled=True),
        shared_down,
        preferred_element_type=jnp.float32,
    )
    expert_out = routed_sum.astype(jnp.bfloat16).reshape(groups, capacity, columns)
    returned = stepwise_exchange(expert_out, EP, (0, 1), 0, 0).reshape(groups * capacity, columns)
    picked = returned[slot_index].astype(jnp.float32) * route_weights.reshape(-1)[:, None]
    moe_sum = jnp.sum(picked.reshape(rows_b, per_row, columns), axis=1) + shared_sum
    return (conv_result, moe_sum.astype(jnp.bfloat16))


def solution(mesh):
    finer = Mesh(mesh.devices.reshape(8, 4, mesh.shape["tp"]), ("ep_0", "ep_1", "tp"))
    in_specs = (
        P(EP, "tp"),
        P(EP, "tp"),
        P(None, "tp"),
        P("tp"),
        P("tp"),
        P(None, "tp"),
        P(EP, None),
        P(),
        P(EP, None),
        P(EP, None),
        P(EP, None, "tp"),
        P(EP, None, "tp"),
        P(EP, None, "tp"),
        P(None, "tp"),
        P(None, "tp"),
        P(None, "tp"),
    )
    out_specs = (P(EP, "tp"), P(EP, "tp"))
    return jax.shard_map(body, mesh=finer, in_specs=in_specs, out_specs=out_specs, check_vma=False)
```

profile of v0, /device:TPU:1, one launch (start us, length us, event | category | flops | bytes accessed | tf_op | source)
XLA Modules:
  0.0 226.3 jit_solution(18367188397835349781)
XLA Ops:
  8.0 0.8 copy.33
  9.0 1.2 fusion.6
  10.5 1.2 reduce-window.6
  12.1 1.2 fusion.8
  13.3 12.8 %scatter_custom_fusion = bf16[1024,2048]{1,0:T(8,128)(2,1)} fusion(s32[512]{0:T(512)S(1)} %bitcast.118, bf16[128,2048]{1,0:T(8,128)(2,1)S(1)} %fusion.8, s32[1024]{0:T(1024)S(1)} %pad_clamp_fusion.1, bf16[]{:T(256)} %constant.47.clone.1), kind=kCustom, calls=%fused_computation.3 | custom fusion | bytes 4194306 | tf_op jit(solution)/shard_map/scatter | solution.py:104
  26.1 1.5 constant_dynamic-slice_fusion
  27.6 24.8 %all_to_all.15 = bf16[32,2,2048]{2,1,0:T(2,128)(2,1)S(1)} all-to-all(bf16[32,2,2048]{2,1,0:T(2,128)(2,1)S(1)} %constant_dynamic-slice_fusion), channel_id=1, replica_groups=mesh['ep_0'=8,'ep_1'=4,'tp'=16] {'ep_0','ep_1'}, dimensions={0} | all-to-all | bytes 524288 | tf_op jit(solution)/shard_map/all_to_all | solution.py:109
  53.3 42.1 %all-gather.6.cloned.1.call-done = bf16[32,32,2048]{2,0,1:T(8,128)(2,1)} async-done(((bf16[32,2,2048]{2,0,1:T(8,128)(2,1)}), bf16[32,32,2048]{2,0,1:T(8,128)(2,1)}) %all-gather.6.cloned.1.call-update) | async-done | bytes 4194320 | tf_op jit(solution)/shard_map/all_gather | solution.py:110
  95.4 4.5 %copy.37 = bf16[32,32,2048]{2,1,0:T(8,128)(2,1)S(1)} copy(bf16[32,32,2048]{2,0,1:T(8,128)(2,1)} %all-gather.6.cloned.1.call-done) | data formatting | bytes 8388608 | tf_op jit(solution)/shard_map/all_gather | solution.py:110
  99.9 1.3 fusion.11
  101.2 2.1 fusion.3
  103.5 3.1 %collective-permute-start = (bf16[30,128]{1,0:T(8,128)(2,1)S(1)}, bf16[30,128]{1,0:T(8,128)(2,1)S(1)}, u32[]{:S(2)}, u32[]{:S(2)}) collective-permute-start(bf16[30,128]{1,0:T(8,128)(2,1)S(1)} %slice.260), channel_id=1, source_target_pairs={{0,16},{16,32},{32,48},{48,64},{64,80},{80,96},{96,112},{112,128},... | collective-permute-start | bytes 23048 | tf_op jit(solution)/shard_map/ppermute | solution.py:13
  107.4 1.2 fusion.47
  108.6 25.0 %all-reduce = (f32[512]{0:T(512)S(1)}, f32[512]{0:T(512)S(1)}) all-reduce(f32[512]{0:T(512)S(1)} %get-tuple-element.3, f32[512]{0:T(512)S(1)} %get-tuple-element.2), channel_id=1, replica_groups=mesh['ep_0'=8,'ep_1'=4,'tp'=16] {'tp'}, use_global_device_ids=true, to_apply=%region_3.0 | all-reduce | flops 1024 | bytes 8192 | tf_op jit(solution)/shard_map/psum | solution.py:70
  133.7 0.9 multiply_convert_fusion
  134.6 35.8 %all-gather.8.cloned.1.call-done = bf16[1024,4096]{1,0:T(8,128)(2,1)} async-done(((bf16[1024,256]{1,0:T(8,128)(2,1)}), bf16[1024,4096]{1,0:T(8,128)(2,1)}) %all-gather.8.cloned.1.call-update) | async-done | bytes 8388624 | tf_op jit(solution)/shard_map/all_gather | solution.py:122
  170.4 6.7 %convolution_convert_fusion = bf16[1024,128]{1,0:T(8,128)(2,1)} fusion(bf16[1024,4096]{1,0:T(8,128)(2,1)} %all-gather.8.cloned.1.call-done, bf16[1,4096,128]{2,1,0:T(8,128)(2,1)} %param.28), kind=kOutput, calls=%fused_computation.39 | convolution fusion | flops 1073872896 | bytes 9699328 | tf_op jit(solution)/shard_map/dot_general | solution.py:121
  177.1 6.5 %all-to-all-start.1 = ((bf16[8,4,1,32,128]{4,3,1,2,0:T(8,128)(2,1)}), bf16[8,4,1,32,128]{4,3,1,2,0:T(8,128)(2,1)S(1)}, u32[]{:S(2)}, u32[]{:S(2)}) async-start(bf16[8,4,1,32,128]{4,3,1,2,0:T(8,128)(2,1)} %bitcast.41), calls=%async_computation.1 | async-start | bytes 524288 | tf_op jit(solution)/shard_map/all_to_all | solution.py:31
  184.3 16.1 %all_gather.15 = bf16[128,512]{0,1:T(8,128)(2,1)S(1)} all-gather(bf16[128,32]{0,1:T(8,128)(2,1)S(1)} %fusion.5), channel_id=1, replica_groups=mesh['ep_0'=8,'ep_1'=4,'tp'=16] {'tp'}, dimensions={1}, use_global_device_ids=true | all-gather | bytes 139264 | tf_op jit(solution)/shard_map/all_gather | solution.py:127
  201.1 4.1 %all-to-all-start.2 = ((bf16[8,4,1,32,128]{4,3,0,2,1:T(8,128)(2,1)}), bf16[8,4,1,32,128]{4,3,0,2,1:T(8,128)(2,1)S(1)}, u32[]{:S(2)}, u32[]{:S(2)}) async-start(bf16[8,4,1,32,128]{4,3,0,2,1:T(8,128)(2,1)} %copy.39), calls=%async_computation.2 | async-start | bytes 524288 | tf_op jit(solution)/shard_map/all_to_all | solution.py:31
  205.2 9.1 %all-gather.4.cloned.1.call-done = bf16[512,2048]{1,0:T(8,128)(2,1)} async-done(((bf16[512,128]{1,0:T(8,128)(2,1)}), bf16[512,2048]{1,0:T(8,128)(2,1)}) %all-gather.4.cloned.1.call-update) | async-done | bytes 2097168 | tf_op jit(solution)/shard_map/all_gather | solution.py:81
  214.3 3.0 %convolution_convert_fusion.1 = bf16[512,128]{1,0:T(8,128)(2,1)} fusion(bf16[512,2048]{1,0:T(8,128)(2,1)} %all-gather.4.cloned.1.call-done, bf16[2048,128]{1,0:T(8,128)(2,1)S(1)} %copy-done.1), kind=kOutput, calls=%fused_computation.40 | convolution fusion | flops 268500992 | bytes 2752512 | tf_op jit(solution)/shard_map/dot_general | solution.py:80
  217.3 1.3 gather_fusion
  218.9 0.8 fusion.4
  (60 shorter events, 5.1 us)
Async XLA Ops:
  7.2 92.7 %copy-start = (bf16[1,2048,256]{2,1,0:T(8,128)(2,1)S(1)}, bf16[1,2048,256]{2,1,0:T(8,128)(2,1)}, u32[]{:S(2)}) copy-start(bf16[1,2048,256]{2,1,0:T(8,128)(2,1)} %param.26) | copy-start | bytes 3145732
  7.2 88.2 %all-gather.6.cloned.1.call-start = ((), (), s32[]{:S(2)}) async-start(), calls=%async_computation.4 | async-start | bytes 4456448 | tf_op jit(solution)/shard_map/all_gather | solution.py:110
  53.2 117.2 %all-gather.8.cloned.1.call-start = ((), (), s32[]{:S(2)}) async-start(), calls=%async_computation.5 | async-start | bytes 8912896 | tf_op jit(solution)/shard_map/all_gather | solution.py:122
  99.9 1.3 copy-start.11
  101.2 2.3 copy-start.2
  101.2 2.3 copy-start.3
  101.2 5.5 %copy-start.7 = (f32[31,128]{1,0:T(8,128)S(1)}, f32[31,128]{1,0:T(8,128)}, u32[]{:S(2)}) copy-start(f32[31,128]{1,0:T(8,128)} %param.18) | copy-start | bytes 47620
  101.2 32.4 %copy-start.9 = (f32[128]{0:T(128)S(1)}, f32[128]{0:T(128)}, u32[]{:S(2)}) copy-start(f32[128]{0:T(128)} %param.20) | copy-start | bytes 1540
  101.2 32.4 %copy-start.10 = (f32[128]{0:T(128)S(1)}, f32[128]{0:T(128)}, u32[]{:S(2)}) copy-start(f32[128]{0:T(128)} %param.19) | copy-start | bytes 1540
  103.4 110.9 %all-gather.4.cloned.1.call-start = ((), (), s32[]{:S(2)}) async-start(), calls=%async_computation.3 | async-start | bytes 2228224 | tf_op jit(solution)/shard_map/all_gather | solution.py:81
  103.5 3.9 %collective-permute-start = (bf16[30,128]{1,0:T(8,128)(2,1)S(1)}, bf16[30,128]{1,0:T(8,128)(2,1)S(1)}, u32[]{:S(2)}, u32[]{:S(2)}) collective-permute-start(bf16[30,128]{1,0:T(8,128)(2,1)S(1)} %slice.260), channel_id=1, source_target_pairs={{0,16},{16,32},{32,48},{48,64},{64,80},{80,96},{96,112},{112,128},... | collective-permute-start | bytes 23048 | tf_op jit(solution)/shard_map/ppermute | solution.py:13
  134.6 49.1 %copy-start.4 = (bf16[2048,32]{0,1:T(8,128)(2,1)S(1)}, bf16[2048,32]{0,1:T(8,128)(2,1)}, u32[]{:S(2)}) copy-start(bf16[2048,32]{0,1:T(8,128)(2,1)} %param.29) | copy-start | bytes 393220
  134.6 49.3 %copy-start.8 = (f32[128,4]{0,1:T(4,128)S(1)}, f32[128,4]{0,1:T(4,128)}, u32[]{:S(2)}) copy-start(f32[128,4]{0,1:T(4,128)} %param.25) | copy-start | bytes 6148
  134.6 49.5 %copy-start.5 = (bf16[2048,32]{0,1:T(8,128)(2,1)S(1)}, bf16[2048,32]{0,1:T(8,128)(2,1)}, u32[]{:S(2)}) copy-start(bf16[2048,32]{0,1:T(8,128)(2,1)} %param.30) | copy-start | bytes 393220
  134.6 79.7 %copy-start.1 = (bf16[2048,128]{1,0:T(8,128)(2,1)S(1)}, bf16[2048,128]{1,0:T(8,128)(2,1)}, u32[]{:S(2)}) copy-start(bf16[2048,128]{1,0:T(8,128)(2,1)} %param.21) | copy-start | bytes 1572868
  177.1 41.8 %copy-start.6 = (bf16[512,128]{1,0:T(8,128)(2,1)S(1)}, bf16[512,128]{1,0:T(8,128)(2,1)}, u32[]{:S(2)}) copy-start(bf16[512,128]{1,0:T(8,128)(2,1)} %param.31) | copy-start | bytes 393220
  177.1 23.3 %all-to-all-start.1 = ((bf16[8,4,1,32,128]{4,3,1,2,0:T(8,128)(2,1)}), bf16[8,4,1,32,128]{4,3,1,2,0:T(8,128)(2,1)S(1)}, u32[]{:S(2)}, u32[]{:S(2)}) async-start(bf16[8,4,1,32,128]{4,3,1,2,0:T(8,128)(2,1)} %bitcast.41), calls=%async_computation.1 | async-start | bytes 524288 | tf_op jit(solution)/shard_map/all_to_all | solution.py:31
  201.1 16.1 %all-to-all-start.2 = ((bf16[8,4,1,32,128]{4,3,0,2,1:T(8,128)(2,1)}), bf16[8,4,1,32,128]{4,3,0,2,1:T(8,128)(2,1)S(1)}, u32[]{:S(2)}, u32[]{:S(2)}) async-start(bf16[8,4,1,32,128]{4,3,0,2,1:T(8,128)(2,1)} %copy.39), calls=%async_computation.2 | async-start | bytes 524288 | tf_op jit(solution)/shard_map/all_to_all | solution.py:31
Sparse Core Ops, SparseCore 0:
  53.3 42.0 all-gather.5
  103.5 66.8 all-gather.7
  173.1 41.1 all-gather.3
where the time goes:
time: 227 us; the launch traced here: 226 us
  waiting for transfers between devices  87.8 us (39%)
  blocking collectives  65.9 us (29%)
  local copies, waits for them, and re-layouts  23.3 us (10%)
  matrix products  14.4 us (6%)
  between operations  14 us (6%)
  starting transfers between devices  13.8 us (6%)
  other arithmetic  6.99 us (3%)
    all_gather x1, waiting for transfers between devices, body(): arrived = lax.all_gather(partial_rows, 'tp', axis=1, tiled=True)  42.1 us
    all_gather x1, waiting for transfers between devices, body(): lax.all_gather(expert_hidden, 'tp', axis=1, tiled=True)  35.8 us
    psum x1, blocking collectives, body(): lax.psum((jnp.sum(filtered, axis=1), jnp.sum(filtered * filtered, axis=1)...  25 us
    all_to_all x1, blocking collectives, body(): lax.all_to_all(own_slots, EP, split_axis=0, concat_axis=0, tiled=True)  24.8 us
    all_gather x1, blocking collectives, body(): lax.all_gather(shared_hidden, 'tp', axis=1, tiled=True)  16.1 us
    scatter x1, local copies, waits for them, and re-layouts, body(): outgoing = jnp.zeros((groups * capacity, model_width), jnp.bfloat16).at[s...  12.8 us
    all_to_all x2, starting transfers between devices, exchange_in_order(): lax.all_to_all(parts, axes[k], split_axis=k, concat_axis=k, tiled=True)  10.6 us
    all_gather x1, waiting for transfers between devices, body(): lax.all_gather(conv_hidden, 'tp', axis=1, tiled=True)  9.08 us
  transfers between devices with their start and end apart: 6, of which 4 were waited for; matrix products, arithmetic and copies ran while one was open for 6% of the time, Pallas kernels for 0%

commit v1 on v0

v1 whole, which is shorter than its diff:
```python
import functools

import jax
import jax.numpy as jnp
from jax import lax
from jax.experimental import pallas as pl
from jax.experimental.pallas import tpu as pltpu
from jax.sharding import PartitionSpec as P

MESH = pl.DeviceIdType.MESH
F32 = jnp.float32
BF16 = jnp.bfloat16

NZ, NX, NY, NC = 8, 4, 8, 2
N_EP, N_TP = NZ * NX, NY * NC
D = 2048
CH = D // N_TP
TAPS = 31
HALO = 32
ROWS_A = 512
TOK = 128
CAP = 32
SLOTS = N_EP * CAP
TOPK = 4
HID = 256
SH = 32
GROUPS = 4
GROWS = SLOTS // GROUPS
CBROWS = ROWS_A + SH


def dot(a, b, dims=(((1,), (0,)), ((), ())), precision=None):
    return lax.dot_general(a, b, dims, precision=precision, preferred_element_type=F32)


NT = (((1,), (1,)), ((), ()))
TN = (((0,), (0,)), ((), ()))


def sigmoid(v):
    return 1.0 / (1.0 + jnp.exp(-v))


def silu(v):
    return v / (1.0 + jnp.exp(-v))


class Ring:
    def __init__(self, place, piece, half, sems, here):
        self.piece, self.half, self.here = piece, half, here
        self.sr, self.sl, self.rr, self.rl, self.ps, self.pr = (s.at[place] for s in sems)
        self.sent = []

    def chip(self, d):
        return lax.rem(self.here["y"] + d + 2 * NY, NY)

    def start(self, ref, send, recv, to):
        copy = pltpu.make_async_remote_copy(
            src_ref=ref, dst_ref=ref, send_sem=send, recv_sem=recv,
            device_id=(self.here["ep"], to), device_id_type=MESH,
        )
        copy.start()
        self.sent.append(copy)

    def wait_at(self, ref, send, recv, frm):
        pltpu.make_async_remote_copy(
            src_ref=ref, dst_ref=ref, send_sem=send, recv_sem=recv,
            device_id=(self.here["ep"], frm), device_id_type=MESH,
        ).wait_recv()

    def at(self, chip, core, part=None):
        t = chip * NC + core
        return self.piece(t) if part is None else self.half(t, part)

    def own(self):
        h = self.here
        mine = self.at(h["y"], h["core"])
        self.start(mine, self.sr.at[0], self.rr.at[0], h["right"])
        self.start(mine, self.sl.at[0], self.rl.at[0], h["left"])
        self.start(mine, self.ps.at[0], self.pr.at[0], h["partner"])

    def stage(self, d):
        h = self.here
        for way, (ss, rs, sign, to, frm) in enumerate(
            ((self.sr, self.rr, -1, h["right"], h["left"]), (self.sl, self.rl, 1, h["left"], h["right"]))
        ):
            chip = self.chip(sign * d)
            got = self.at(chip, h["core"], way if d == 4 else None)
            self.wait_at(got, ss.at[d - 1], rs.at[d - 1], frm)
            if d < 3:
                self.start(got, ss.at[d], rs.at[d], to)
            elif d == 3:
                self.start(self.at(chip, h["core"], way), ss.at[3], rs.at[3], to)
            k = 1 + way * 4 + (d - 1)
            self.start(got, self.ps.at[k], self.pr.at[k], h["partner"])

    def from_partner(self, d):
        h = self.here
        if d == 0:
            self.wait_at(self.at(h["y"], 1 - h["core"]), self.ps.at[0], self.pr.at[0], h["partner"])
            return
        for way, sign in enumerate((-1, 1)):
            got = self.at(self.chip(sign * d), 1 - h["core"], way if d == 4 else None)
            k = 1 + way * 4 + (d - 1)
            self.wait_at(got, self.ps.at[k], self.pr.at[k], h["partner"])

    def drain(self):
        for copy in self.sent:
            copy.wait_send()


def kernel(
    value_h, gate_h, taps_h, gain_h, shift_h, wc_h, x_h, mgain_h, routes_h, rw_h, wg_h, wu_h, wd_h, sg_h, su_h, sd_h,
    conv_o, moe_o,
    value, gate, taps, gain, shift, wc, x, mgain, routes, rw, wg, wu, wd, sg, su, sd,
    pad, halo_out, halo_in, filt, stat, normed, slot, wslot, onehot, packed, chi, clo,
    dbuf, hbuf, cbuf, gacc, uacc, oacc, outb, rbuf,
    load, misc, sr, sl, rr, rl, ps, pr,
):
    ep, tp = lax.axis_index("ep"), lax.axis_index("tp")
    z, xx = lax.div(ep, NX), lax.rem(ep, NX)
    y, core = lax.div(tp, NC), lax.rem(tp, NC)
    here = {
        "ep": ep, "y": y, "core": core,
        "right": lax.rem(y + 1, NY) * NC + core,
        "left": lax.rem(y + NY - 1, NY) * NC + core,
        "partner": y * NC + (1 - core),
    }

    def peer(rho, sign):
        q, dx = lax.div(rho, NX), lax.rem(rho, NX)
        odd = lax.rem(q, 2)
        dz = odd * lax.div(q + 1, 2) + (1 - odd) * lax.rem(NZ - lax.div(q, 2), NZ)
        return lax.rem(z + sign * dz + NZ, NZ) * NX + lax.rem(xx + sign * dx + NX, NX)

    loads = [
        pltpu.make_async_copy(a, b, load.at[i])
        for i, (a, b) in enumerate(
            (
                (x_h, x), (mgain_h, mgain), (routes_h, routes), (value_h, value), (gate_h, gate), (taps_h, taps),
                (gain_h, gain), (shift_h, shift), (sg_h, sg), (su_h, su), (wg_h, wg), (wu_h, wu), (wc_h, wc),
                (wd_h, wd), (rw_h, rw), (sd_h, sd),
            )
        )
    ]
    for copy in loads:
        copy.start()

    barrier = pltpu.get_barrier_semaphore()

    def greet_tp(r, carry):
        pl.semaphore_signal(barrier, inc=1, device_id=(ep, lax.rem(tp + r, N_TP)), device_id_type=MESH)
        return carry

    def greet_ep(r, carry):
        pl.semaphore_signal(barrier, inc=1, device_id=(lax.rem(ep + r, N_EP), tp), device_id_type=MESH)
        return carry

    lax.fori_loop(1, N_TP, greet_tp, 0)
    lax.fori_loop(1, N_EP, greet_ep, 0)

    for i in range(3):
        loads[i].wait()
    for r in range(0, TOK, 32):
        rows = x[r : r + 32, :].astype(F32)
        mean = jnp.mean(rows * rows, axis=1, keepdims=True)
        normed[r : r + 32, :] = (rows * lax.rsqrt(mean + 1e-06) * mgain[...]).astype(BF16)
    rho = lax.broadcasted_iota(jnp.int32, (N_EP, TOK), 0)
    q, dx = rho >> 2, rho & 3
    dz = jnp.where((q & 1) == 1, (q + 1) >> 1, (NZ - (q >> 1)) & 7)
    expert = ((z + dz) & 7) * NX + ((xx + dx) & 3)
    hits = jnp.zeros((N_EP, TOK), F32)
    for k in range(TOPK):
        hits = hits + jnp.where(routes[k : k + 1, :] == expert, 1.0, 0.0)
    before = jnp.where(
        lax.broadcasted_iota(jnp.int32, (TOK, TOK), 0) < lax.broadcasted_iota(jnp.int32, (TOK, TOK), 1), 1.0, 0.0
    ).astype(BF16)
    rank = dot(hits.astype(BF16), before)
    slot[...] = jnp.where(hits > 0.5, rank, -1.0)
    place = lax.broadcasted_iota(jnp.int32, (CAP, TOK), 0).astype(F32)
    for r in range(N_EP):
        onehot[r * CAP : (r + 1) * CAP, :] = jnp.where(slot[r : r + 1, :] == place, 1.0, 0.0).astype(BF16)
    mine = normed[:, pl.ds(pl.multiple_of(tp * CH, CH), CH)]
    packed[...] = dot(onehot[...], mine).astype(BF16)

    loads[3].wait()
    loads[4].wait()
    glu = (value[...].astype(F32) * sigmoid(gate[...].astype(F32))).astype(BF16)
    pad[HALO:, :] = glu.astype(F32)
    halo_out[...] = glu[ROWS_A - HALO :, :]

    pl.semaphore_wait(barrier, N_TP - 1 + N_EP - 1)

    def dispatch(r, carry):
        pltpu.make_async_remote_copy(
            src_ref=packed.at[pl.ds(r * CAP, CAP)], dst_ref=dbuf.at[tp, pl.ds(r * CAP, CAP)],
            send_sem=misc.at[0], recv_sem=misc.at[1], device_id=(peer(r, 1), tp), device_id_type=MESH,
        ).start()
        return carry

    halo = pltpu.make_async_remote_copy(
        src_ref=halo_out, dst_ref=halo_in, send_sem=misc.at[2], recv_sem=misc.at[3],
        device_id=(lax.rem(ep + 1, N_EP), tp), device_id_type=MESH,
    )
    halo.start()
    lax.fori_loop(1, N_EP, dispatch, 0)
    dbuf[tp, 0:CAP, :] = packed[0:CAP, :]

    loads[8].wait()
    loads[9].wait()
    shared = silu(dot(sg[...], normed[...], NT)) * dot(su[...], normed[...], NT)
    cbuf[tp, ROWS_A:, :] = shared.astype(BF16)

    loads[5].wait()
    loads[6].wait()
    loads[7].wait()
    halo.wait_recv()
    pad[:HALO, :] = halo_in[...].astype(F32) * jnp.where(ep > 0, 1.0, 0.0)
    for b in range(0, ROWS_A, 64):
        total = jnp.zeros((64, CH), F32)
        for j in range(TAPS):
            first = b + j + HALO - (TAPS - 1)
            total = total + taps[j : j + 1, :] * pad[first : first + 64, :]
        filt[b : b + 64, :] = total
    ones = jnp.ones((8, CH), F32)
    for r in range(4):
        part = filt[r * 128 : (r + 1) * 128, :]
        stat[0, r : r + 1, :] = dot(ones, part, NT, lax.Precision.HIGHEST)[0:1, :]
        stat[0, 4 + r : 5 + r, :] = dot(ones, part * part, NT, lax.Precision.HIGHEST)[0:1, :]

    def sums(r, carry):
        pltpu.make_async_remote_copy(
            src_ref=stat.at[0], dst_ref=stat.at[r], send_sem=misc.at[4], recv_sem=misc.at[5],
            device_id=(ep, lax.rem(tp + r, N_TP)), device_id_type=MESH,
        ).start()
        return carry

    lax.fori_loop(1, N_TP, sums, 0)

    sems = (sr, sl, rr, rl, ps, pr)
    ring_d = Ring(
        0, lambda t: dbuf.at[t], lambda t, i: dbuf.at[t, pl.ds(i * (SLOTS // 2), SLOTS // 2)], sems, here
    )
    ring_c = Ring(
        1, lambda t: cbuf.at[t], lambda t, i: cbuf.at[t, pl.ds(i * (CBROWS // 2), CBROWS // 2)], sems, here
    )
    ring_h = [
        Ring(
            2 + g,
            lambda t, g=g: hbuf.at[t, pl.ds(g * GROWS, GROWS)],
            lambda t, i, g=g: hbuf.at[t, pl.ds(g * GROWS + i * (GROWS // 2), GROWS // 2)],
            sems, here,
        )
        for g in range(GROUPS)
    ]

    arrived = pltpu.make_async_remote_copy(
        src_ref=packed.at[pl.ds(CAP, SLOTS - CAP)], dst_ref=dbuf.at[tp, pl.ds(CAP, SLOTS - CAP)],
        send_sem=misc.at[0], recv_sem=misc.at[1], device_id=(ep, here["right"]), device_id_type=MESH,
    )
    arrived.wait_recv()
    ring_d.own()

    summed = pltpu.make_async_remote_copy(
        src_ref=stat.at[pl.ds(1, N_TP - 1)], dst_ref=stat.at[pl.ds(1, N_TP - 1)],
        send_sem=misc.at[4], recv_sem=misc.at[5], device_id=(ep, here["right"]), device_id_type=MESH,
    )
    summed.wait_recv()
    total = stat[0]
    for r in range(1, N_TP):
        total = total + stat[r]
    total = total * (1.0 / D)
    mean, square = total[0:4, :], total[4:8, :]
    scale = lax.rsqrt(square - mean * mean + 1e-05)
    turned = jnp.concatenate([mean, scale], axis=0).T
    for r in range(4):
        part = filt[r * 128 : (r + 1) * 128, :]
        part = (part - turned[:, r : r + 1]) * turned[:, 4 + r : 5 + r]
        cbuf[tp, r * 128 : (r + 1) * 128, :] = silu(part * gain[...] + shift[...]).astype(BF16)
    ring_c.own()

    def gate_up(chip, g, first):
        rows = pl.ds(pl.multiple_of(g * GROWS, GROWS), GROWS)
        lhs = jnp.concatenate([dbuf[chip * NC, rows, :], dbuf[chip * NC + 1, rows, :]], axis=1)
        depth = pl.ds(pl.multiple_of(chip * NC * CH, NC * CH), NC * CH)
        a, b = dot(lhs, wg[depth, :]), dot(lhs, wu[depth, :])
        if first:
            gacc[rows, :] = a
            uacc[rows, :] = b
        else:
            gacc[rows, :] += a
            uacc[rows, :] += b

    def all_groups(chip, first=False):
        def step(g, carry):
            gate_up(chip, g, first)
            return carry

        lax.fori_loop(0, GROUPS, step, 0)

    loads[10].wait()
    loads[11].wait()
    ring_d.from_partner(0)
    all_groups(y, True)
    for d in range(1, 4):
        ring_d.stage(d)
        ring_c.stage(d)
        ring_d.from_partner(d)
        all_groups(ring_d.chip(-d))
        all_groups(ring_d.chip(d))

    def hidden(g):
        gate_up(ring_d.chip(4), g, False)
        rows = slice(g * GROWS, (g + 1) * GROWS)
        hbuf[tp, rows, :] = (silu(gacc[rows, :]) * uacc[rows, :]).astype(BF16)

    ring_d.stage(4)
    ring_d.from_partner(4)
    hidden(3)
    ring_h[3].own()
    hidden(2)
    ring_h[2].own()
    ring_c.stage(4)
    hidden(1)
    hidden(0)

    loads[14].wait()
    weight = jnp.zeros((N_EP, TOK), F32)
    for k in range(TOPK):
        weight = weight + jnp.where(routes[k : k + 1, :] == expert, rw[k : k + 1, :], 0.0)
    wslot[...] = weight
    for r in range(N_EP):
        w = wslot[r : r + 1, :]
        high = w.astype(BF16).astype(F32)
        hot = onehot[r * CAP : (r + 1) * CAP, :].astype(F32)
        chi[r * CAP : (r + 1) * CAP, :] = (hot * high).astype(BF16)
        clo[r * CAP : (r + 1) * CAP, :] = (hot * (w - high)).astype(BF16)

    loads[13].wait()

    def down(g, chip, first):
        rows = slice(g * GROWS, (g + 1) * GROWS)
        lhs = jnp.concatenate([hbuf[chip * NC, rows, :], hbuf[chip * NC + 1, rows, :]], axis=1)
        depth = pl.ds(pl.multiple_of(chip * NC * HID, NC * HID), NC * HID)
        a = dot(lhs, wd[depth, :])
        if first:
            oacc[rows, :] = a
        else:
            oacc[rows, :] += a

    def give_back(g):
        rows = slice(g * GROWS, (g + 1) * GROWS)
        outb[rows, :] = oacc[rows, :].astype(BF16)

        def back(r, carry):
            pltpu.make_async_remote_copy(
                src_ref=outb.at[pl.ds(r * CAP, CAP)], dst_ref=rbuf.at[pl.ds(r * CAP, CAP)],
                send_sem=misc.at[6], recv_sem=misc.at[7], device_id=(peer(r, -1), tp), device_id_type=MESH,
            ).start()
            return carry

        per = GROWS // CAP
        lax.fori_loop(max(1, g * per), (g + 1) * per, back, 0)

    def h_stage(g, d):
        ring_h[g].stage(d)
        ring_h[g].from_partner(d)
        if d < 4:
            down(g, ring_d.chip(-d), False)
        down(g, ring_d.chip(d), False)

    for pair in ((3, 2), (1, 0)):
        for g in pair:
            ring_h[g].from_partner(0)
            down(g, y, True)
        for d in range(1, 5):
            for i, g in enumerate(pair):
                h_stage(g, d)
                if d == 3 and pair == (3, 2):
                    ring_h[1 - i].own()
                if d == 4:
                    give_back(g)
        if pair == (3, 2):
            loads[12].wait()
            for d in range(5):
                ring_c.from_partner(d)
            for b in range(0, ROWS_A, 256):
                total = jnp.zeros((256, CH), F32)
                for t in range(0, N_TP, 2):
                    lhs = jnp.concatenate([cbuf[t, b : b + 256, :], cbuf[t + 1, b : b + 256, :]], axis=1)
                    total = total + dot(lhs, wc[t * CH : (t + 2) * CH, :])
                conv_o[b : b + 256, :] = total.astype(BF16)

    loads[15].wait()
    mid = jnp.concatenate([cbuf[t, ROWS_A:, :] for t in range(N_TP)], axis=0)
    shared_sum = dot(mid, sd[...], TN)
    rbuf[0:CAP, :] = outb[0:CAP, :]
    returned = pltpu.make_async_remote_copy(
        src_ref=outb.at[pl.ds(CAP, SLOTS - CAP)], dst_ref=rbuf.at[pl.ds(CAP, SLOTS - CAP)],
        send_sem=misc.at[6], recv_sem=misc.at[7], device_id=(ep, here["right"]), device_id_type=MESH,
    )
    returned.wait_recv()
    moe_o[...] = (dot(chi[...], rbuf[...], TN) + dot(clo[...], rbuf[...], TN) + shared_sum).astype(BF16)

    arrived.wait_send()
    halo.wait_send()
    summed.wait_send()
    returned.wait_send()
    for ring in (ring_d, ring_c, *ring_h):
        ring.drain()


def body(*args):
    (
        conv_value, conv_gate, conv_taps, norm_gain, norm_shift, conv_out_weight, moe_input, moe_gain, routes,
        route_weights, expert_gate, expert_up, expert_down, shared_gate, shared_up, shared_down,
    ) = args
    operands = (
        conv_value, conv_gate, conv_taps, norm_gain.reshape(1, CH), norm_shift.reshape(1, CH), conv_out_weight,
        moe_input, moe_gain.reshape(1, D), routes.T, route_weights.T, expert_gate[0], expert_up[0], expert_down[0],
        shared_gate.T, shared_up.T, shared_down,
    )
    vmem = pltpu.VMEM
    dma = pltpu.SemaphoreType.DMA
    rings = 2 + GROUPS
    return pl.pallas_call(
        kernel,
        out_shape=(jax.ShapeDtypeStruct((ROWS_A, CH), BF16), jax.ShapeDtypeStruct((TOK, CH), BF16)),
        in_specs=[pl.BlockSpec(memory_space=pl.ANY)] * len(operands),
        out_specs=(pl.BlockSpec(memory_space=pltpu.VMEM),) * 2,
        scratch_shapes=[vmem(o.shape, o.dtype) for o in operands]
        + [
            vmem((HALO + ROWS_A, CH), F32),
            vmem((HALO, CH), BF16),
            vmem((HALO, CH), BF16),
            vmem((ROWS_A, CH), F32),
            vmem((N_TP, 8, CH), F32),
            vmem((TOK, D), BF16),
            vmem((N_EP, TOK), F32),
            vmem((N_EP, TOK), F32),
            vmem((SLOTS, TOK), BF16),
            vmem((SLOTS, CH), BF16),
            vmem((SLOTS, TOK), BF16),
            vmem((SLOTS, TOK), BF16),
            vmem((N_TP, SLOTS, CH), BF16),
            vmem((N_TP, SLOTS, HID), BF16),
            vmem((N_TP, CBROWS, CH), BF16),
            vmem((SLOTS, HID), F32),
            vmem((SLOTS, HID), F32),
            vmem((SLOTS, CH), F32),
            vmem((SLOTS, CH), BF16),
            vmem((SLOTS, CH), BF16),
            dma((16,)),
            dma((8,)),
            dma((rings, 4)),
            dma((rings, 4)),
            dma((rings, 4)),
            dma((rings, 4)),
            dma((rings, 9)),
            dma((rings, 9)),
        ],
        compiler_params=pltpu.CompilerParams(
            collective_id=0, has_side_effects=True, vmem_limit_bytes=56 * 1024 * 1024
        ),
        cost_estimate=pl.CostEstimate(flops=5_000_000_000, bytes_accessed=8_000_000, transcendentals=0),
    )(*operands)


def solution(mesh):
    in_specs = (
        P("ep", "tp"),
        P("ep", "tp"),
        P(None, "tp"),
        P("tp"),
        P("tp"),
        P(None, "tp"),
        P("ep", None),
        P(),
        P("ep", None),
        P("ep", None),
        P("ep", None, "tp"),
        P("ep", None, "tp"),
        P("ep", None, "tp"),
        P(None, "tp"),
        P(None, "tp"),
        P(None, "tp"),
    )
    out_specs = (P("ep", "tp"), P("ep", "tp"))
    return jax.shard_map(body, mesh=mesh, in_specs=in_specs, out_specs=out_specs, check_vma=False)
```

time: 227 us -> 114 us (0.50)
  Pallas kernels: 0 us -> 111 us
  waiting for transfers between devices: 87.8 us -> 0 us
  blocking collectives: 65.9 us -> 0 us
  local copies, waits for them, and re-layouts: 23.3 us -> 2.19 us
  matrix products: 14.4 us -> 0 us
  starting transfers between devices: 13.8 us -> 0 us
  between operations: 14 us -> 0.65 us
  other arithmetic: 6.99 us -> 0 us
    pallas_call x0 -> x1, Pallas kernels: none -> 111 us  [body(): pl.pallas_call(kernel, out_shape=(jax.ShapeDtypeStruct((ROWS_A, CH), BF16...]
    all_gather x3 -> x0, waiting for transfers between devices: 87 us -> none  [the longest x1 42.1 us: body(): arrived = lax.all_gather(partial_rows, 'tp', axis=1, tiled=True)]
    psum x1 -> x0, blocking collectives: 25 us -> none  [body(): lax.psum((jnp.sum(filtered, axis=1), jnp.sum(filtered * filtered, axis=1)...]
    all_to_all x1 -> x0, blocking collectives: 24.8 us -> none  [body(): lax.all_to_all(own_slots, EP, split_axis=0, concat_axis=0, tiled=True)]
    all_gather x1 -> x0, blocking collectives: 16.1 us -> none  [body(): lax.all_gather(shared_hidden, 'tp', axis=1, tiled=True)]
    dot_general x7 -> x0, matrix products: 14.4 us -> none  [the longest x1 6.66 us: body(): jnp.dot(lax.all_gather(expert_hidden, 'tp', axis=1, tiled=True), routed_r...]
    scatter x1 -> x0, local copies, waits for them, and re-layouts: 12.8 us -> none  [body(): outgoing = jnp.zeros((groups * capacity, model_width), jnp.bfloat16).at[s...]
    all_to_all x2 -> x0, starting transfers between devices: 10.6 us -> none  [exchange_in_order(): lax.all_to_all(parts, axes[k], split_axis=k, concat_axis=k, tiled=True)]
  transfers between devices with their start and end apart: 6 -> 0, of which waited for: 4 -> 0; matrix products, arithmetic and copies ran while one was open for 6% -> 0% of each run, Pallas kernels for 0% -> 0%
where the time goes in v1:
time: 114 us
  Pallas kernels  111 us (97%)
  local copies, waits for them, and re-layouts  2.19 us (2%)
    pallas_call x1, Pallas kernels, body(): pl.pallas_call(kernel, out_shape=(jax.ShapeDtypeStruct((ROWS_A, CH), BF16...  111 us

profile of v1, /device:TPU:1, one launch (start us, length us, event | category | flops | bytes accessed | tf_op | source)
XLA Modules:
  0.0 113.8 jit_solution(555470860208041141)
XLA Ops:
  0.6 111.0 %shard_map.167 = (bf16[512,128]{1,0:T(8,128)(2,1)}, bf16[128,128]{1,0:T(8,128)(2,1)}) custom-call(bf16[512,128]{1,0:T(8,128)(2,1)} %value_h.1, bf16[512,128]{1,0:T(8,128)(2,1)} %gate_h.1, f32[31,128]{1,0:T(8,128)} %taps_h.1, f32[1,128]{1,0:T(1,128)} %bitcast.18, f32[1,128]{1,0:T(1,128)} %bitcast.19, bf16[2048,128]{1,0:T(8,128)(2,1)} %wc_h.1, ...), custom_call_target="tpu_custom_call" | custom-call | flops 5000000000 | bytes 8000000 | tf_op jit(solution)/shard_map/pallas_call | solution.py:426
  111.6 0.0 copy-start
  111.6 1.6 %copy.20 = bf16[512,128]{1,0:T(8,128)(2,1)} copy(bf16[512,128]{1,0:T(8,128)(2,1)} %get-tuple-element.4) | data formatting | bytes 262144
  113.2 0.0 copy-done
  113.2 0.6 copy.21
Async XLA Ops:
  111.6 1.6 %copy-start = (bf16[128,128]{1,0:T(8,128)(2,1)S(1)}, bf16[128,128]{1,0:T(8,128)(2,1)}, u32[]{:S(2)}) copy-start(bf16[128,128]{1,0:T(8,128)(2,1)} %get-tuple-element.5) | copy-start | bytes 98308

commit v2 on v1

--- a/solution.py
+++ b/solution.py
@@ -24,8 +24,13 @@
 TOPK = 4
 HID = 256
 SH = 32
-GROUPS = 4
-GROWS = SLOTS // GROUPS
+QROWS = NX * CAP
+NEAR = 5
+NEAR_BLOCKS = NEAR * NX
+NEAR_ROWS = NEAR * QROWS
+FAR_ROWS = SLOTS - NEAR_ROWS
+WIDE = D // NC
+GROUPS = ((0, 256), (512, 256), (768, 256), (384, 128), (256, 128))
 CBROWS = ROWS_A + SH
 
 
@@ -111,11 +116,11 @@
 
 def kernel(
     value_h, gate_h, taps_h, gain_h, shift_h, wc_h, x_h, mgain_h, routes_h, rw_h, wg_h, wu_h, wd_h, sg_h, su_h, sd_h,
-    conv_o, moe_o,
-    value, gate, taps, gain, shift, wc, x, mgain, routes, rw, wg, wu, wd, sg, su, sd,
-    pad, halo_out, halo_in, filt, stat, normed, slot, wslot, onehot, packed, chi, clo,
-    dbuf, hbuf, cbuf, gacc, uacc, oacc, outb, rbuf,
-    load, misc, sr, sl, rr, rl, ps, pr,
+    conv_h, moe_h,
+    value, gate, taps, gain, shift, wc, x, mgain, routes, rw, wg, wu, wd, sg, su, sd, conv_o, moe_o,
+    pad, halo_out, halo_in, filt, stat, normed, slot, wslot, onehot, wide, packed, chi, clo,
+    nbuf, dbuf, hbuf, cbuf, oacc, outb, rbuf,
+    load, misc, near_s, near_r, sr, sl, rr, rl, ps, pr,
 ):
     ep, tp = lax.axis_index("ep"), lax.axis_index("tp")
     z, xx = lax.div(ep, NX), lax.rem(ep, NX)
@@ -132,6 +137,11 @@
         odd = lax.rem(q, 2)
         dz = odd * lax.div(q + 1, 2) + (1 - odd) * lax.rem(NZ - lax.div(q, 2), NZ)
         return lax.rem(z + sign * dz + NZ, NZ) * NX + lax.rem(xx + sign * dx + NX, NX)
+
+    def remote(src, dst, send, recv, to_ep, to_tp):
+        return pltpu.make_async_remote_copy(
+            src_ref=src, dst_ref=dst, send_sem=send, recv_sem=recv, device_id=(to_ep, to_tp), device_id_type=MESH
+        )
 
     loads = [
         pltpu.make_async_copy(a, b, load.at[i])
@@ -181,7 +191,16 @@
     for r in range(N_EP):
         onehot[r * CAP : (r + 1) * CAP, :] = jnp.where(slot[r : r + 1, :] == place, 1.0, 0.0).astype(BF16)
     mine = normed[:, pl.ds(pl.multiple_of(tp * CH, CH), CH)]
-    packed[...] = dot(onehot[...], mine).astype(BF16)
+    packed[...] = dot(onehot[NEAR_ROWS:, :], mine).astype(BF16)
+    mine = normed[:, pl.ds(pl.multiple_of(core * WIDE, WIDE), WIDE)]
+
+    def pack(i, carry):
+        rows = pl.ds(pl.multiple_of(i * QROWS, QROWS), QROWS)
+        wide[rows, :] = dot(onehot[rows, :], mine).astype(BF16)
+        return carry
+
+    lax.fori_loop(0, NEAR, pack, 0)
+    nbuf[core, 0:CAP, :] = wide[0:CAP, :]
 
     loads[3].wait()
     loads[4].wait()
@@ -192,19 +211,23 @@
     pl.semaphore_wait(barrier, N_TP - 1 + N_EP - 1)
 
     def dispatch(r, carry):
-        pltpu.make_async_remote_copy(
-            src_ref=packed.at[pl.ds(r * CAP, CAP)], dst_ref=dbuf.at[tp, pl.ds(r * CAP, CAP)],
-            send_sem=misc.at[0], recv_sem=misc.at[1], device_id=(peer(r, 1), tp), device_id_type=MESH,
-        ).start()
+        rows = pl.ds((r - NEAR_BLOCKS) * CAP, CAP)
+        remote(packed.at[rows], dbuf.at[tp, rows], misc.at[0], misc.at[1], peer(r, 1), tp).start()
         return carry
 
-    halo = pltpu.make_async_remote_copy(
-        src_ref=halo_out, dst_ref=halo_in, send_sem=misc.at[2], recv_sem=misc.at[3],
-        device_id=(lax.rem(ep + 1, N_EP), tp), device_id_type=MESH,
-    )
+    def dispatch_near(q):
+        def step(r, carry):
+            rows = pl.ds(r * CAP, CAP)
+            remote(wide.at[rows], nbuf.at[core, rows], near_s.at[q], near_r.at[q], peer(r, 1), tp).start()
+            return carry
+
+        lax.fori_loop(max(1, q * NX), (q + 1) * NX, step, 0)
+
+    halo = remote(halo_out, halo_in, misc.at[2], misc.at[3], lax.rem(ep + 1, N_EP), tp)
     halo.start()
-    lax.fori_loop(1, N_EP, dispatch, 0)
-    dbuf[tp, 0:CAP, :] = packed[0:CAP, :]
+    lax.fori_loop(NEAR_BLOCKS, N_EP, dispatch, 0)
+    for q in range(NEAR):
+        dispatch_near(q)
 
     loads[8].wait()
     loads[9].wait()
@@ -229,17 +252,14 @@
         stat[0, 4 + r : 5 + r, :] = dot(ones, part * part, NT, lax.Precision.HIGHEST)[0:1, :]
 
     def sums(r, carry):
-        pltpu.make_async_remote_copy(
-            src_ref=stat.at[0], dst_ref=stat.at[r], send_sem=misc.at[4], recv_sem=misc.at[5],
-            device_id=(ep, lax.rem(tp + r, N_TP)), device_id_type=MESH,
-        ).start()
+        remote(stat.at[0], stat.at[r], misc.at[4], misc.at[5], ep, lax.rem(tp + r, N_TP)).start()
         return carry
 
     lax.fori_loop(1, N_TP, sums, 0)
 
     sems = (sr, sl, rr, rl, ps, pr)
     ring_d = Ring(
-        0, lambda t: dbuf.at[t], lambda t, i: dbuf.at[t, pl.ds(i * (SLOTS // 2), SLOTS // 2)], sems, here
+        0, lambda t: dbuf.at[t], lambda t, i: dbuf.at[t, pl.ds(i * (FAR_ROWS // 2), FAR_ROWS // 2)], sems, here
     )
     ring_c = Ring(
         1, lambda t: cbuf.at[t], lambda t, i: cbuf.at[t, pl.ds(i * (CBROWS // 2), CBROWS // 2)], sems, here
@@ -247,24 +267,19 @@
     ring_h = [
         Ring(
             2 + g,
-            lambda t, g=g: hbuf.at[t, pl.ds(g * GROWS, GROWS)],
-            lambda t, i, g=g: hbuf.at[t, pl.ds(g * GROWS + i * (GROWS // 2), GROWS // 2)],
+            lambda t, a=a, n=n: hbuf.at[t, pl.ds(a, n)],
+            lambda t, i, a=a, n=n: hbuf.at[t, pl.ds(a + i * (n // 2), n // 2)],
             sems, here,
         )
-        for g in range(GROUPS)
+        for g, (a, n) in enumerate(GROUPS)
     ]
 
-    arrived = pltpu.make_async_remote_copy(
-        src_ref=packed.at[pl.ds(CAP, SLOTS - CAP)], dst_ref=dbuf.at[tp, pl.ds(CAP, SLOTS - CAP)],
-        send_sem=misc.at[0], recv_sem=misc.at[1], device_id=(ep, here["right"]), device_id_type=MESH,
-    )
+    arrived = remote(packed, dbuf.at[tp], misc.at[0], misc.at[1], ep, here["right"])
     arrived.wait_recv()
     ring_d.own()
 
-    summed = pltpu.make_async_remote_copy(
-        src_ref=stat.at[pl.ds(1, N_TP - 1)], dst_ref=stat.at[pl.ds(1, N_TP - 1)],
-        send_sem=misc.at[4], recv_sem=misc.at[5], device_id=(ep, here["right"]), device_id_type=MESH,
-    )
+    rest = pl.ds(1, N_TP - 1)
+    summed = remote(stat.at[rest], stat.at[rest], misc.at[4], misc.at[5], ep, here["right"])
     summed.wait_recv()
     total = stat[0]
     for r in range(1, N_TP):
@@ -279,50 +294,109 @@
         cbuf[tp, r * 128 : (r + 1) * 128, :] = silu(part * gain[...] + shift[...]).astype(BF16)
     ring_c.own()
 
-    def gate_up(chip, g, first):
-        rows = pl.ds(pl.multiple_of(g * GROWS, GROWS), GROWS)
-        lhs = jnp.concatenate([dbuf[chip * NC, rows, :], dbuf[chip * NC + 1, rows, :]], axis=1)
-        depth = pl.ds(pl.multiple_of(chip * NC * CH, NC * CH), NC * CH)
-        a, b = dot(lhs, wg[depth, :]), dot(lhs, wu[depth, :])
+    passed = []
+    landed = []
+
+    def take_near(q):
+        first = max(CAP, q * QROWS)
+        rows = pl.ds(first, (q + 1) * QROWS - first)
+        copy = remote(wide.at[rows], nbuf.at[core, rows], near_s.at[q], near_r.at[q], ep, here["right"])
+        copy.wait_recv()
+        landed.append(copy)
+        rows = pl.ds(q * QROWS, QROWS)
+        copy = remote(
+            nbuf.at[core, rows], nbuf.at[core, rows], near_s.at[NEAR + q], near_r.at[NEAR + q], ep, here["partner"]
+        )
+        copy.start()
+        passed.append(copy)
+
+    def near_from_partner(q):
+        rows = pl.ds(q * QROWS, QROWS)
+        remote(
+            nbuf.at[1 - core, rows], nbuf.at[1 - core, rows], near_s.at[NEAR + q], near_r.at[NEAR + q],
+            ep, here["partner"],
+        ).wait_recv()
+
+    def hidden(q):
+        if q < NEAR:
+            near_from_partner(q)
+            rows = slice(q * QROWS, (q + 1) * QROWS)
+            a = dot(nbuf[0, rows, :], wg[:WIDE, :]) + dot(nbuf[1, rows, :], wg[WIDE:, :])
+            b = dot(nbuf[0, rows, :], wu[:WIDE, :]) + dot(nbuf[1, rows, :], wu[WIDE:, :])
+        else:
+            rows = slice((q - NEAR) * QROWS, (q - NEAR + 1) * QROWS)
+            lhs = jnp.concatenate([dbuf[t, rows, :] for t in range(N_TP)], axis=1)
+            a, b = dot(lhs, wg[...]), dot(lhs, wu[...])
+        hbuf[tp, q * QROWS : (q + 1) * QROWS, :] = (silu(a) * b).astype(BF16)
+
+    def down(g, chip, first):
+        a, n = GROUPS[g]
+        rows = slice(a, a + n)
+        lhs = jnp.concatenate([hbuf[chip * NC, rows, :], hbuf[chip * NC + 1, rows, :]], axis=1)
+        depth = pl.ds(pl.multiple_of(chip * NC * HID, NC * HID), NC * HID)
+        a = dot(lhs, wd[depth, :])
         if first:
-            gacc[rows, :] = a
-            uacc[rows, :] = b
+            oacc[rows, :] = a
         else:
-            gacc[rows, :] += a
-            uacc[rows, :] += b
-
-    def all_groups(chip, first=False):
-        def step(g, carry):
-            gate_up(chip, g, first)
+            oacc[rows, :] += a
+
+    def give_back(g):
+        a, n = GROUPS[g]
+        outb[a : a + n, :] = oacc[a : a + n, :].astype(BF16)
+
+        def back(r, carry):
+            rows = pl.ds(r * CAP, CAP)
+            remote(outb.at[rows], rbuf.at[rows], misc.at[6], misc.at[7], peer(r, -1), tp).start()
             return carry
 
-        lax.fori_loop(0, GROUPS, step, 0)
-
+        lax.fori_loop(max(1, a // CAP), (a + n) // CAP, back, 0)
+
+    def h_own(g):
+        ring_h[g].from_partner(0)
+        down(g, y, True)
+
+    def h_stage(g, d):
+        ring_h[g].stage(d)
+        ring_h[g].from_partner(d)
+        if d < 4:
+            down(g, ring_d.chip(-d), False)
+        down(g, ring_d.chip(d), False)
+
+    take_near(0)
+    take_near(1)
+    ring_d.stage(1)
+    ring_c.stage(1)
     loads[10].wait()
     loads[11].wait()
-    ring_d.from_partner(0)
-    all_groups(y, True)
-    for d in range(1, 4):
-        ring_d.stage(d)
-        ring_c.stage(d)
+    hidden(0)
+    hidden(1)
+    ring_h[0].own()
+    ring_d.stage(2)
+    ring_c.stage(2)
+    loads[13].wait()
+    h_own(0)
+    h_stage(0, 1)
+    take_near(2)
+    take_near(3)
+    ring_d.stage(3)
+    ring_c.stage(3)
+    h_stage(0, 2)
+    take_near(4)
+    ring_d.stage(4)
+    h_stage(0, 3)
+    for d in range(5):
         ring_d.from_partner(d)
-        all_groups(ring_d.chip(-d))
-        all_groups(ring_d.chip(d))
-
-    def hidden(g):
-        gate_up(ring_d.chip(4), g, False)
-        rows = slice(g * GROWS, (g + 1) * GROWS)
-        hbuf[tp, rows, :] = (silu(gacc[rows, :]) * uacc[rows, :]).astype(BF16)
-
-    ring_d.stage(4)
-    ring_d.from_partner(4)
-    hidden(3)
-    ring_h[3].own()
-    hidden(2)
+    hidden(4)
+    hidden(5)
+    ring_h[1].own()
+    hidden(6)
+    hidden(7)
     ring_h[2].own()
     ring_c.stage(4)
-    hidden(1)
-    hidden(0)
+    h_stage(0, 4)
+    give_back(0)
+    hidden(2)
+    hidden(3)
 
     loads[14].wait()
     weight = jnp.zeros((N_EP, TOK), F32)
@@ -336,51 +410,17 @@
         chi[r * CAP : (r + 1) * CAP, :] = (hot * high).astype(BF16)
         clo[r * CAP : (r + 1) * CAP, :] = (hot * (w - high)).astype(BF16)
 
-    loads[13].wait()
-
-    def down(g, chip, first):
-        rows = slice(g * GROWS, (g + 1) * GROWS)
-        lhs = jnp.concatenate([hbuf[chip * NC, rows, :], hbuf[chip * NC + 1, rows, :]], axis=1)
-        depth = pl.ds(pl.multiple_of(chip * NC * HID, NC * HID), NC * HID)
-        a = dot(lhs, wd[depth, :])
-        if first:
-            oacc[rows, :] = a
-        else:
-            oacc[rows, :] += a
-
-    def give_back(g):
-        rows = slice(g * GROWS, (g + 1) * GROWS)
-        outb[rows, :] = oacc[rows, :].astype(BF16)
-
-        def back(r, carry):
-            pltpu.make_async_remote_copy(
-                src_ref=outb.at[pl.ds(r * CAP, CAP)], dst_ref=rbuf.at[pl.ds(r * CAP, CAP)],
-                send_sem=misc.at[6], recv_sem=misc.at[7], device_id=(peer(r, -1), tp), device_id_type=MESH,
-            ).start()
-            return carry
-
-        per = GROWS // CAP
-        lax.fori_loop(max(1, g * per), (g + 1) * per, back, 0)
-
-    def h_stage(g, d):
-        ring_h[g].stage(d)
-        ring_h[g].from_partner(d)
-        if d < 4:
-            down(g, ring_d.chip(-d), False)
-        down(g, ring_d.chip(d), False)
-
-    for pair in ((3, 2), (1, 0)):
+    for pair in ((1, 2), (3, 4)):
         for g in pair:
-            ring_h[g].from_partner(0)
-            down(g, y, True)
+            h_own(g)
         for d in range(1, 5):
             for i, g in enumerate(pair):
                 h_stage(g, d)
-                if d == 3 and pair == (3, 2):
-                    ring_h[1 - i].own()
+                if d == 3 and pair == (1, 2):
+                    ring_h[3 + i].own()
                 if d == 4:
                     give_back(g)
-        if pair == (3, 2):
+        if pair == (1, 2):
             loads[12].wait()
             for d in range(5):
                 ring_c.from_partner(d)
@@ -390,24 +430,26 @@
                     lhs = jnp.concatenate([cbuf[t, b : b + 256, :], cbuf[t + 1, b : b + 256, :]], axis=1)
                     total = total + dot(lhs, wc[t * CH : (t + 2) * CH, :])
                 conv_o[b : b + 256, :] = total.astype(BF16)
-
-    loads[15].wait()
-    mid = jnp.concatenate([cbuf[t, ROWS_A:, :] for t in range(N_TP)], axis=0)
-    shared_sum = dot(mid, sd[...], TN)
+            conv_out = pltpu.make_async_copy(conv_o, conv_h, load.at[16])
+            conv_out.start()
+            loads[15].wait()
+            mid = jnp.concatenate([cbuf[t, ROWS_A:, :] for t in range(N_TP)], axis=0)
+            shared_sum = dot(mid, sd[...], TN)
+
     rbuf[0:CAP, :] = outb[0:CAP, :]
-    returned = pltpu.make_async_remote_copy(
-        src_ref=outb.at[pl.ds(CAP, SLOTS - CAP)], dst_ref=rbuf.at[pl.ds(CAP, SLOTS - CAP)],
-        send_sem=misc.at[6], recv_sem=misc.at[7], device_id=(ep, here["right"]), device_id_type=MESH,
-    )
+    rest = pl.ds(CAP, SLOTS - CAP)
+    returned = remote(outb.at[rest], rbuf.at[rest], misc.at[6], misc.at[7], ep, here["right"])
     returned.wait_recv()
     moe_o[...] = (dot(chi[...], rbuf[...], TN) + dot(clo[...], rbuf[...], TN) + shared_sum).astype(BF16)
-
-    arrived.wait_send()
-    halo.wait_send()
-    summed.wait_send()
-    returned.wait_send()
+    moe_out = pltpu.make_async_copy(moe_o, moe_h, load.at[17])
+    moe_out.start()
+
+    for copy in (arrived, halo, summed, returned, *landed, *passed):
+        copy.wait_send()
     for ring in (ring_d, ring_c, *ring_h):
         ring.drain()
+    conv_out.wait()
+    moe_out.wait()
 
 
 def body(*args):
@@ -422,13 +464,14 @@
     )
     vmem = pltpu.VMEM
     dma = pltpu.SemaphoreType.DMA
-    rings = 2 + GROUPS
+    rings = 2 + len(GROUPS)
+    outs = (jax.ShapeDtypeStruct((ROWS_A, CH), BF16), jax.ShapeDtypeStruct((TOK, CH), BF16))
     return pl.pallas_call(
         kernel,
-        out_shape=(jax.ShapeDtypeStruct((ROWS_A, CH), BF16), jax.ShapeDtypeStruct((TOK, CH), BF16)),
+        out_shape=outs,
         in_specs=[pl.BlockSpec(memory_space=pl.ANY)] * len(operands),
-        out_specs=(pl.BlockSpec(memory_space=pltpu.VMEM),) * 2,
-        scratch_shapes=[vmem(o.shape, o.dtype) for o in operands]
+        out_specs=(pl.BlockSpec(memory_space=pl.ANY),) * 2,
+        scratch_shapes=[vmem(o.shape, o.dtype) for o in (*operands, *outs)]
         + [
             vmem((HALO + ROWS_A, CH), F32),
             vmem((HALO, CH), BF16),
@@ -439,19 +482,21 @@
             vmem((N_EP, TOK), F32),
             vmem((N_EP, TOK), F32),
             vmem((SLOTS, TOK), BF16),
-            vmem((SLOTS, CH), BF16),
+            vmem((NEAR_ROWS, WIDE), BF16),
+            vmem((FAR_ROWS, CH), BF16),
             vmem((SLOTS, TOK), BF16),
             vmem((SLOTS, TOK), BF16),
-            vmem((N_TP, SLOTS, CH), BF16),
+            vmem((NC, NEAR_ROWS, WIDE), BF16),
+            vmem((N_TP, FAR_ROWS, CH), BF16),
             vmem((N_TP, SLOTS, HID), BF16),
             vmem((N_TP, CBROWS, CH), BF16),
-            vmem((SLOTS, HID), F32),
-            vmem((SLOTS, HID), F32),
             vmem((SLOTS, CH), F32),
             vmem((SLOTS, CH), BF16),
             vmem((SLOTS, CH), BF16),
-            dma((16,)),
+            dma((18,)),
             dma((8,)),
+            dma((2 * NEAR,)),
+            dma((2 * NEAR,)),
             dma((rings, 4)),
             dma((rings, 4)),
             dma((rings, 4)),

time: 114 us -> 106 us (0.930)
  Pallas kernels: 111 us -> 103 us
    pallas_call x1, Pallas kernels: 111 us -> 103 us  [body(): pl.pallas_call(kernel, out_shape=outs, in_specs=[pl.BlockSpec(memory_spac...]
where the time goes in v2:
time: 106 us
  Pallas kernels  103 us (97%)
  local copies, waits for them, and re-layouts  2.19 us (2%)
    pallas_call x1, Pallas kernels, body(): pl.pallas_call(kernel, out_shape=outs, in_specs=[pl.BlockSpec(memory_spac...  103 us
    unnamed x4, local copies, waits for them, and re-layouts  2.19 us

profile of v2, /device:TPU:1, one launch (start us, length us, event | category | flops | bytes accessed | tf_op | source)
XLA Modules:
  0.0 106.2 jit_solution(13002798742566973330)
XLA Ops:
  0.6 103.4 %shard_map.167 = (bf16[512,128]{1,0:T(8,128)(2,1)}, bf16[128,128]{1,0:T(8,128)(2,1)}) custom-call(bf16[512,128]{1,0:T(8,128)(2,1)} %value_h.1, bf16[512,128]{1,0:T(8,128)(2,1)} %gate_h.1, f32[31,128]{1,0:T(8,128)} %taps_h.1, f32[1,128]{1,0:T(1,128)} %bitcast.18, f32[1,128]{1,0:T(1,128)} %bitcast.19, bf16[2048,128]{1,0:T(8,128)(2,1)} %wc_h.1, ...), custom_call_target="tpu_custom_call" | custom-call | flops 5000000000 | bytes 8000000 | tf_op jit(solution)/shard_map/pallas_call | solution.py:469
  104.0 0.0 copy-start
  104.0 1.6 %copy.20 = bf16[512,128]{1,0:T(8,128)(2,1)} copy(bf16[512,128]{1,0:T(8,128)(2,1)} %get-tuple-element.4) | data formatting | bytes 262144
  105.6 0.0 copy-done
  105.6 0.6 copy.21
Async XLA Ops:
  104.0 1.6 %copy-start = (bf16[128,128]{1,0:T(8,128)(2,1)S(1)}, bf16[128,128]{1,0:T(8,128)(2,1)}, u32[]{:S(2)}) copy-start(bf16[128,128]{1,0:T(8,128)(2,1)} %get-tuple-element.5) | copy-start | bytes 98308

commit v3 on v2

v3 whole, which is shorter than its diff:
```python
import functools

import jax
import jax.numpy as jnp
from jax import lax
from jax.experimental import pallas as pl
from jax.experimental.pallas import tpu as pltpu
from jax.sharding import PartitionSpec as P

MESH = pl.DeviceIdType.MESH
F32 = jnp.float32
BF16 = jnp.bfloat16

NZ, NX, NY, NC = 8, 4, 8, 2
N_EP, N_TP = NZ * NX, NY * NC
D = 2048
CH = D // N_TP
TAPS = 31
HALO = 32
ROWS_A = 512
TOK = 128
CAP = 32
SLOTS = N_EP * CAP
TOPK = 4
HID = 256
SH = 32
QROWS = NX * CAP
NEAR = 5
NEAR_BLOCKS = NEAR * NX
NEAR_ROWS = NEAR * QROWS
FAR_ROWS = SLOTS - NEAR_ROWS
WIDE = D // NC
GROUPS = ((0, 128), (640, 384), (384, 256), (128, 256))
CBROWS = ROWS_A + SH
CSPLIT = ROWS_A // 2


def dot(a, b, dims=(((1,), (0,)), ((), ())), precision=None):
    return lax.dot_general(a, b, dims, precision=precision, preferred_element_type=F32)


NT = (((1,), (1,)), ((), ()))
TN = (((0,), (0,)), ((), ()))


def sigmoid(v):
    return 1.0 / (1.0 + jnp.exp(-v))


def silu(v):
    return v / (1.0 + jnp.exp(-v))


class Ring:
    def __init__(self, place, buffer, first, rows, sems, here):
        self.buffer, self.first, self.rows, self.here = buffer, first, rows, here
        send, rr, rl, pr = sems
        self.send = send.at[place]
        self.rr, self.rl, self.pr = rr.at[place], rl.at[place], pr.at[place]

    def chip(self, d):
        return lax.rem(self.here["y"] + d + 2 * NY, NY)

    def remote(self, ref, recv, to):
        return pltpu.make_async_remote_copy(
            src_ref=ref, dst_ref=ref, send_sem=self.send, recv_sem=recv,
            device_id=(self.here["ep"], to), device_id_type=MESH,
        )

    def at(self, chip, core, part=None):
        if part is None:
            return self.buffer.at[chip * NC + core, pl.ds(self.first, self.rows)]
        half = self.rows // 2
        return self.buffer.at[chip * NC + core, pl.ds(self.first + part * half, half)]

    def many(self, n):
        return self.buffer.at[pl.ds(0, n), pl.ds(self.first, self.rows)]

    def own(self):
        h = self.here
        mine = self.at(h["y"], h["core"])
        self.remote(mine, self.rr.at[0], h["right"]).start()
        self.remote(mine, self.rl.at[0], h["left"]).start()
        self.remote(mine, self.pr.at[0], h["partner"]).start()

    def stage(self, d):
        h = self.here
        for way, (rs, sign, to) in enumerate(((self.rr, -1, h["right"]), (self.rl, 1, h["left"]))):
            chip = self.chip(sign * d)
            got = self.at(chip, h["core"], way if d == 4 else None)
            self.remote(got, rs.at[d - 1], to).wait_recv()
            if d < 3:
                self.remote(got, rs.at[d], to).start()
            elif d == 3:
                self.remote(self.at(chip, h["core"], way), rs.at[3], to).start()
            self.remote(got, self.pr.at[d], h["partner"]).start()

    def from_partner(self, d):
        got = self.many(2 if 0 < d < 4 else 1)
        self.remote(got, self.pr.at[d], self.here["partner"]).wait_recv()

    def drain(self):
        self.remote(self.many(N_TP - 1), self.pr.at[0], self.here["partner"]).wait_send()


def kernel(
    value_h, gate_h, taps_h, gain_h, shift_h, wc_h, x_h, mgain_h, routes_h, rw_h, wg_h, wu_h, wd_h, sg_h, su_h, sd_h,
    conv_o, moe_o,
    value, gate, taps, gain, shift, wc, x, mgain, routes, rw, wg, wu, wd, sg, su, sd,
    pad, halo_out, halo_in, filt, stat, normed, slot, wslot, onehot, wide, packed, chi, clo,
    nbuf, dbuf, hbuf, cbuf, oacc, outb, rbuf,
    load, misc, near_s, near_r, back_s, back_r, send, rr, rl, pr,
):
    ep, tp = lax.axis_index("ep"), lax.axis_index("tp")
    z, xx = lax.div(ep, NX), lax.rem(ep, NX)
    y, core = lax.div(tp, NC), lax.rem(tp, NC)
    here = {
        "ep": ep, "y": y, "core": core,
        "right": lax.rem(y + 1, NY) * NC + core,
        "left": lax.rem(y + NY - 1, NY) * NC + core,
        "partner": y * NC + (1 - core),
    }

    def peer(rho, sign):
        q, dx = lax.div(rho, NX), lax.rem(rho, NX)
        odd = lax.rem(q, 2)
        dz = odd * lax.div(q + 1, 2) + (1 - odd) * lax.rem(NZ - lax.div(q, 2), NZ)
        return lax.rem(z + sign * dz + NZ, NZ) * NX + lax.rem(xx + sign * dx + NX, NX)

    def remote(src, dst, send, recv, to_ep, to_tp):
        return pltpu.make_async_remote_copy(
            src_ref=src, dst_ref=dst, send_sem=send, recv_sem=recv, device_id=(to_ep, to_tp), device_id_type=MESH
        )

    loads = [
        pltpu.make_async_copy(a, b, load.at[i])
        for i, (a, b) in enumerate(
            (
                (x_h, x), (mgain_h, mgain), (routes_h, routes), (value_h, value), (gate_h, gate), (taps_h, taps),
                (gain_h, gain), (shift_h, shift), (sg_h, sg), (su_h, su), (wg_h, wg), (wu_h, wu), (wc_h, wc),
                (wd_h, wd), (rw_h, rw), (sd_h, sd),
            )
        )
    ]
    for copy in loads[:5]:
        copy.start()

    barrier = pltpu.get_barrier_semaphore()

    def greet_tp(r, carry):
        pl.semaphore_signal(barrier, inc=1, device_id=(ep, lax.rem(tp + r, N_TP)), device_id_type=MESH)
        return carry

    def greet_ep(r, carry):
        pl.semaphore_signal(barrier, inc=1, device_id=(lax.rem(ep + r, N_EP), tp), device_id_type=MESH)
        return carry

    lax.fori_loop(1, N_EP, greet_ep, 0)
    lax.fori_loop(1, N_TP, greet_tp, 0)

    for copy in loads[5:]:
        copy.start()

    for i in range(3):
        loads[i].wait()
    for r in range(0, TOK, 32):
        rows = x[r : r + 32, :].astype(F32)
        mean = jnp.mean(rows * rows, axis=1, keepdims=True)
        normed[r : r + 32, :] = (rows * lax.rsqrt(mean + 1e-06) * mgain[...]).astype(BF16)
    rho = lax.broadcasted_iota(jnp.int32, (N_EP, TOK), 0)
    q, dx = rho >> 2, rho & 3
    dz = jnp.where((q & 1) == 1, (q + 1) >> 1, (NZ - (q >> 1)) & 7)
    expert = ((z + dz) & 7) * NX + ((xx + dx) & 3)
    hits = jnp.zeros((N_EP, TOK), F32)
    for k in range(TOPK):
        hits = hits + jnp.where(routes[k : k + 1, :] == expert, 1.0, 0.0)
    before = jnp.where(
        lax.broadcasted_iota(jnp.int32, (TOK, TOK), 0) < lax.broadcasted_iota(jnp.int32, (TOK, TOK), 1), 1.0, 0.0
    ).astype(BF16)
    rank = dot(hits.astype(BF16), before)
    slot[...] = jnp.where(hits > 0.5, rank, -1.0)
    place = lax.broadcasted_iota(jnp.int32, (CAP, TOK), 0).astype(F32)
    for r in range(N_EP):
        onehot[r * CAP : (r + 1) * CAP, :] = jnp.where(slot[r : r + 1, :] == place, 1.0, 0.0).astype(BF16)

    def pack(q):
        rows = slice(q * QROWS, (q + 1) * QROWS)
        mine = normed[:, pl.ds(pl.multiple_of(core * WIDE, WIDE), WIDE)]
        wide[rows, :] = dot(onehot[rows, :], mine).astype(BF16)

    pack(0)

    loads[3].wait()
    loads[4].wait()
    glu = (value[...].astype(F32) * sigmoid(gate[...].astype(F32))).astype(BF16)
    pad[HALO:, :] = glu.astype(F32)
    halo_out[...] = glu[ROWS_A - HALO :, :]
    halo = remote(halo_out, halo_in, misc.at[2], misc.at[3], lax.rem(ep + 1, N_EP), tp)
    pl.semaphore_wait(barrier, N_TP - 1 + N_EP - 1)

    def dispatch(r, carry):
        rows = pl.ds((r - NEAR_BLOCKS) * CAP, CAP)
        remote(packed.at[rows], dbuf.at[tp, rows], misc.at[0], misc.at[1], peer(r, 1), tp).start()
        return carry

    def dispatch_near(q):
        def step(r, carry):
            rows = pl.ds(r * CAP, CAP)
            remote(wide.at[rows], nbuf.at[core, rows], near_s.at[q], near_r.at[q], peer(r, 1), tp).start()
            return carry

        lax.fori_loop(max(1, q * NX), (q + 1) * NX, step, 0)

    @pl.when(ep < N_EP - 1)
    def _():
        halo.start()

    dispatch_near(0)
    nbuf[core, 0:CAP, :] = wide[0:CAP, :]
    packed[...] = dot(onehot[NEAR_ROWS:, :], normed[:, pl.ds(pl.multiple_of(tp * CH, CH), CH)]).astype(BF16)
    lax.fori_loop(NEAR_BLOCKS, N_EP, dispatch, 0)
    for q in (1, 2):
        pack(q)
        dispatch_near(q)

    loads[8].wait()
    loads[9].wait()
    shared = silu(dot(sg[...], normed[...], NT)) * dot(su[...], normed[...], NT)
    cbuf[tp, ROWS_A:, :] = shared.astype(BF16)

    loads[5].wait()
    loads[6].wait()
    loads[7].wait()
    pad[:HALO, :] = jnp.zeros((HALO, CH), F32)

    @pl.when(ep > 0)
    def _():
        halo.wait_recv()
        pad[:HALO, :] = halo_in[...].astype(F32)

    for b in range(0, ROWS_A, 64):
        total = jnp.zeros((64, CH), F32)
        for j in range(TAPS):
            first = b + j + HALO - (TAPS - 1)
            total = total + taps[j : j + 1, :] * pad[first : first + 64, :]
        filt[b : b + 64, :] = total
    ones = jnp.ones((8, CH), F32)
    for r in range(4):
        part = filt[r * 128 : (r + 1) * 128, :]
        stat[0, r : r + 1, :] = dot(ones, part, NT, lax.Precision.HIGHEST)[0:1, :]
        stat[0, 4 + r : 5 + r, :] = dot(ones, part * part, NT, lax.Precision.HIGHEST)[0:1, :]

    def sums(r, carry):
        remote(stat.at[0], stat.at[r], misc.at[4], misc.at[5], ep, lax.rem(tp + r, N_TP)).start()
        return carry

    lax.fori_loop(1, N_TP, sums, 0)

    sems = (send, rr, rl, pr)
    ring_d = Ring(0, dbuf, 0, FAR_ROWS, sems, here)
    ring_c = [Ring(1, cbuf, 0, CSPLIT, sems, here), Ring(2, cbuf, CSPLIT, CBROWS - CSPLIT, sems, here)]
    ring_h = [Ring(3 + g, hbuf, a, n, sems, here) for g, (a, n) in enumerate(GROUPS)]

    passed = []
    landed = []

    def take_near(q):
        first = max(CAP, q * QROWS)
        rows = pl.ds(first, (q + 1) * QROWS - first)
        copy = remote(wide.at[rows], nbuf.at[core, rows], near_s.at[q], near_r.at[q], ep, here["right"])
        copy.wait_recv()
        landed.append(copy)
        rows = pl.ds(q * QROWS, QROWS)
        copy = remote(
            nbuf.at[core, rows], nbuf.at[core, rows], near_s.at[NEAR + q], near_r.at[NEAR + q], ep, here["partner"]
        )
        copy.start()
        passed.append(copy)

    def near_from_partner(q):
        rows = pl.ds(q * QROWS, QROWS)
        remote(
            nbuf.at[1 - core, rows], nbuf.at[1 - core, rows], near_s.at[NEAR + q], near_r.at[NEAR + q],
            ep, here["partner"],
        ).wait_recv()

    def hidden(q):
        if q < NEAR:
            near_from_partner(q)
            rows = slice(q * QROWS, (q + 1) * QROWS)
            a = dot(nbuf[0, rows, :], wg[:WIDE, :]) + dot(nbuf[1, rows, :], wg[WIDE:, :])
            b = dot(nbuf[0, rows, :], wu[:WIDE, :]) + dot(nbuf[1, rows, :], wu[WIDE:, :])
        else:
            rows = slice((q - NEAR) * QROWS, (q - NEAR + 1) * QROWS)
            lhs = jnp.concatenate([dbuf[t, rows, :] for t in range(N_TP)], axis=1)
            a, b = dot(lhs, wg[...]), dot(lhs, wu[...])
        hbuf[tp, q * QROWS : (q + 1) * QROWS, :] = (silu(a) * b).astype(BF16)

    def down(g, chip, first):
        a, n = GROUPS[g]
        rows = slice(a, a + n)
        lhs = jnp.concatenate([hbuf[chip * NC, rows, :], hbuf[chip * NC + 1, rows, :]], axis=1)
        depth = pl.ds(pl.multiple_of(chip * NC * HID, NC * HID), NC * HID)
        a = dot(lhs, wd[depth, :])
        if first:
            oacc[rows, :] = a
        else:
            oacc[rows, :] += a

    def returned(g):
        first, end = max(CAP, GROUPS[g][0]), sum(GROUPS[g])
        rows = pl.ds(first, end - first)
        return remote(outb.at[rows], rbuf.at[rows], back_s.at[g], back_r.at[g], ep, here["right"])

    def combine(g):
        returned(g).wait_recv()
        a, n = GROUPS[g]
        rows = slice(a, a + n)
        return dot(chi[rows, :], rbuf[rows, :], TN) + dot(clo[rows, :], rbuf[rows, :], TN)

    def give_back(g):
        a, n = GROUPS[g]
        outb[a : a + n, :] = oacc[a : a + n, :].astype(BF16)

        def back(r, carry):
            rows = pl.ds(r * CAP, CAP)
            remote(outb.at[rows], rbuf.at[rows], back_s.at[g], back_r.at[g], peer(r, -1), tp).start()
            return carry

        lax.fori_loop(max(1, a // CAP), (a + n) // CAP, back, 0)

    def h_down(g, d):
        ring_h[g].from_partner(d)
        if d < 4:
            down(g, ring_d.chip(-d), d == 0)
        if d > 0:
            down(g, ring_d.chip(d), False)

    def conv_down(part, d):
        ring_c[part].from_partner(d)
        rows = slice(part * CSPLIT, (part + 1) * CSPLIT)
        for sign in (-1, 1)[0 if 0 < d < 4 else 1 :]:
            chip = ring_d.chip(sign * d)
            depth = pl.ds(pl.multiple_of(chip * NC * CH, NC * CH), NC * CH)
            lhs = jnp.concatenate([cbuf[chip * NC, rows, :], cbuf[chip * NC + 1, rows, :]], axis=1)
            product = dot(lhs, wc[depth, :])
            if d == 0:
                filt[rows, :] = product
            else:
                filt[rows, :] += product

    take_near(0)
    loads[10].wait()
    loads[11].wait()
    hidden(0)
    ring_h[0].own()
    arrived = remote(packed, dbuf.at[tp], misc.at[0], misc.at[1], ep, here["right"])
    arrived.wait_recv()
    ring_d.own()
    rest = pl.ds(1, N_TP - 1)
    summed = remote(stat.at[rest], stat.at[rest], misc.at[4], misc.at[5], ep, here["right"])
    summed.wait_recv()
    total = stat[0]
    for r in range(1, N_TP):
        total = total + stat[r]
    total = total * (1.0 / D)
    mean, square = total[0:4, :], total[4:8, :]
    scale = lax.rsqrt(square - mean * mean + 1e-05)
    turned = jnp.concatenate([mean, scale], axis=0).T
    for r in range(4):
        part = filt[r * 128 : (r + 1) * 128, :]
        part = (part - turned[:, r : r + 1]) * turned[:, 4 + r : 5 + r]
        cbuf[tp, r * 128 : (r + 1) * 128, :] = silu(part * gain[...] + shift[...]).astype(BF16)
    ring_c[0].own()
    ring_h[0].stage(1)
    ring_d.stage(1)
    ring_c[0].stage(1)
    loads[13].wait()
    h_down(0, 0)
    take_near(1)
    take_near(2)
    pack(3)
    dispatch_near(3)
    pack(4)
    dispatch_near(4)
    hidden(1)
    hidden(2)
    ring_h[3].own()
    ring_h[0].stage(2)
    ring_d.stage(2)
    ring_c[0].stage(2)
    h_down(0, 1)
    ring_h[0].stage(3)
    ring_d.stage(3)
    ring_c[0].stage(3)
    ring_h[3].stage(1)
    h_down(0, 2)
    h_down(3, 0)
    ring_d.stage(4)
    ring_h[0].stage(4)
    ring_c[0].stage(4)
    ring_h[3].stage(2)
    for d in range(5):
        ring_d.from_partner(d)
    hidden(5)
    hidden(6)
    hidden(7)
    ring_h[1].own()
    h_down(0, 3)
    h_down(0, 4)
    give_back(0)
    take_near(3)
    take_near(4)
    hidden(3)
    hidden(4)
    ring_h[2].own()
    ring_h[3].stage(3)
    h_down(3, 1)
    h_down(3, 2)
    ring_h[1].stage(1)
    ring_h[3].stage(4)
    ring_h[2].stage(1)
    h_down(3, 3)
    h_down(3, 4)
    give_back(3)
    h_down(1, 0)
    h_down(2, 0)
    ring_h[1].stage(2)
    ring_h[2].stage(2)
    ring_c[1].own()
    h_down(1, 1)
    h_down(2, 1)
    loads[12].wait()
    for d in range(5):
        conv_down(0, d)
    ring_h[1].stage(3)
    ring_h[2].stage(3)
    ring_c[1].stage(1)
    h_down(1, 2)
    h_down(2, 2)

    loads[14].wait()
    weight = jnp.zeros((N_EP, TOK), F32)
    for k in range(TOPK):
        weight = weight + jnp.where(routes[k : k + 1, :] == expert, rw[k : k + 1, :], 0.0)
    wslot[...] = weight
    for r in range(N_EP):
        w = wslot[r : r + 1, :]
        high = w.astype(BF16).astype(F32)
        hot = onehot[r * CAP : (r + 1) * CAP, :].astype(F32)
        chi[r * CAP : (r + 1) * CAP, :] = (hot * high).astype(BF16)
        clo[r * CAP : (r + 1) * CAP, :] = (hot * (w - high)).astype(BF16)
    ring_h[1].stage(4)
    ring_h[2].stage(4)
    ring_c[1].stage(2)
    h_down(1, 3)
    h_down(1, 4)
    give_back(1)
    h_down(2, 3)
    h_down(2, 4)
    give_back(2)
    ring_c[1].stage(3)
    for d in range(3):
        conv_down(1, d)
    loads[15].wait()

    rbuf[0:CAP, :] = outb[0:CAP, :]
    summed_up = combine(0) + combine(3)
    ring_c[1].stage(4)
    conv_down(1, 3)
    conv_down(1, 4)
    conv_o[...] = filt[...].astype(BF16)
    mid = jnp.concatenate([cbuf[t, ROWS_A:, :] for t in range(N_TP)], axis=0)
    summed_up = summed_up + dot(mid, sd[...], TN)
    moe_o[...] = (summed_up + combine(1) + combine(2)).astype(BF16)

    @pl.when(ep < N_EP - 1)
    def _():
        halo.wait_send()

    for copy in (arrived, summed, *[returned(g) for g in range(len(GROUPS))], *landed, *passed):
        copy.wait_send()
    for ring in (ring_d, *ring_c, *ring_h):
        ring.drain()


def body(*args):
    (
        conv_value, conv_gate, conv_taps, norm_gain, norm_shift, conv_out_weight, moe_input, moe_gain, routes,
        route_weights, expert_gate, expert_up, expert_down, shared_gate, shared_up, shared_down,
    ) = args
    operands = (
        conv_value, conv_gate, conv_taps, norm_gain.reshape(1, CH), norm_shift.reshape(1, CH), conv_out_weight,
        moe_input, moe_gain.reshape(1, D), routes.T, route_weights.T, expert_gate[0], expert_up[0], expert_down[0],
        shared_gate.T, shared_up.T, shared_down,
    )
    vmem = pltpu.VMEM
    dma = pltpu.SemaphoreType.DMA
    rings = 3 + len(GROUPS)
    outs = (vmem((ROWS_A, CH), BF16), vmem((TOK, CH), BF16))
    return pl.pallas_call(
        kernel,
        out_shape=outs,
        in_specs=[pl.BlockSpec(memory_space=pltpu.HBM)] * len(operands),
        out_specs=(pl.BlockSpec(memory_space=pltpu.VMEM),) * 2,
        scratch_shapes=[vmem(o.shape, o.dtype) for o in operands]
        + [
            vmem((HALO + ROWS_A, CH), F32),
            vmem((HALO, CH), BF16),
            vmem((HALO, CH), BF16),
            vmem((ROWS_A, CH), F32),
            vmem((N_TP, 8, CH), F32),
            vmem((TOK, D), BF16),
            vmem((N_EP, TOK), F32),
            vmem((N_EP, TOK), F32),
            vmem((SLOTS, TOK), BF16),
            vmem((NEAR_ROWS, WIDE), BF16),
            vmem((FAR_ROWS, CH), BF16),
            vmem((SLOTS, TOK), BF16),
            vmem((SLOTS, TOK), BF16),
            vmem((NC, NEAR_ROWS, WIDE), BF16),
            vmem((N_TP, FAR_ROWS, CH), BF16),
            vmem((N_TP, SLOTS, HID), BF16),
            vmem((N_TP, CBROWS, CH), BF16),
            vmem((SLOTS, CH), F32),
            vmem((SLOTS, CH), BF16),
            vmem((SLOTS, CH), BF16),
            dma((16,)),
            dma((6,)),
            dma((2 * NEAR,)),
            dma((2 * NEAR,)),
            dma((len(GROUPS),)),
            dma((len(GROUPS),)),
            dma((rings,)),
            dma((rings, 4)),
            dma((rings, 4)),
            dma((rings, 5)),
        ],
        compiler_params=pltpu.CompilerParams(
            collective_id=0, has_side_effects=True, vmem_limit_bytes=55 * 1024 * 1024
        ),
        cost_estimate=pl.CostEstimate(flops=5_000_000_000, bytes_accessed=8_000_000, transcendentals=0),
    )(*operands)


def solution(mesh):
    in_specs = (
        P("ep", "tp"),
        P("ep", "tp"),
        P(None, "tp"),
        P("tp"),
        P("tp"),
        P(None, "tp"),
        P("ep", None),
        P(),
        P("ep", None),
        P("ep", None),
        P("ep", None, "tp"),
        P("ep", None, "tp"),
        P("ep", None, "tp"),
        P(None, "tp"),
        P(None, "tp"),
        P(None, "tp"),
    )
    out_specs = (P("ep", "tp"), P("ep", "tp"))
    return jax.shard_map(body, mesh=mesh, in_specs=in_specs, out_specs=out_specs, check_vma=False)
```

time: 106 us -> 96.9 us (0.914); the launches traced: 106 us -> 96 us
  Pallas kernels: 103 us -> 94.1 us
    pallas_call x1, Pallas kernels: 103 us -> 94.1 us  [body(): pl.pallas_call(kernel, out_shape=outs, in_specs=[pl.BlockSpec(memory_spac...]
    unnamed x4 -> x2, local copies, waits for them, and re-layouts: 2.19 us -> 1.27 us
where the time goes in v3:
time: 96.9 us; the launch traced here: 96 us
  Pallas kernels  94.1 us (97%)
  local copies, waits for them, and re-layouts  1.27 us (1%)
    pallas_call x1, Pallas kernels, body(): pl.pallas_call(kernel, out_shape=outs, in_specs=[pl.BlockSpec(memory_spac...  94.1 us

profile of v3, /device:TPU:1, one launch (start us, length us, event | category | flops | bytes accessed | tf_op | source)
XLA Modules:
  0.0 96.0 jit_solution(11068412920753881230)
XLA Ops:
  0.6 94.1 %shard_map.167 = (bf16[512,128]{1,0:T(8,128)(2,1)S(1)}, bf16[128,128]{1,0:T(8,128)(2,1)S(1)}) custom-call(bf16[512,128]{1,0:T(8,128)(2,1)} %value_h.1, bf16[512,128]{1,0:T(8,128)(2,1)} %gate_h.1, f32[31,128]{1,0:T(8,128)} %taps_h.1, f32[1,128]{1,0:T(1,128)} %bitcast.18, f32[1,128]{1,0:T(1,128)} %bitcast.19, bf16[2048,128]{1,0:T(8,128)(2,1)} %wc_h.1, ...), custom_call_target="tpu_custom_call" | custom-call | flops 5000000000 | bytes 8000000 | tf_op jit(solution)/shard_map/pallas_call | solution.py:501
  94.7 0.7 copy.20
  95.4 0.6 copy.21

commit v4 on v3

--- a/solution.py
+++ b/solution.py
@@ -54,12 +54,14 @@
 class Ring:
     def __init__(self, place, buffer, first, rows, sems, here):
         self.buffer, self.first, self.rows, self.here = buffer, first, rows, here
-        send, rr, rl, pr = sems
-        self.send = send.at[place]
-        self.rr, self.rl, self.pr = rr.at[place], rl.at[place], pr.at[place]
+        send, recv, pr = sems
+        self.send, self.recv, self.pr = send.at[place], recv.at[place], pr.at[place]
 
     def chip(self, d):
         return lax.rem(self.here["y"] + d + 2 * NY, NY)
+
+    def behind(self, d):
+        return lax.rem(self.here["y"] - self.here["way"] * d + 2 * NY, NY)
 
     def remote(self, ref, recv, to):
         return pltpu.make_async_remote_copy(
@@ -67,11 +69,12 @@
             device_id=(self.here["ep"], to), device_id_type=MESH,
         )
 
-    def at(self, chip, core, part=None):
-        if part is None:
+    def at(self, chip, core, halved=False):
+        if not halved:
             return self.buffer.at[chip * NC + core, pl.ds(self.first, self.rows)]
         half = self.rows // 2
-        return self.buffer.at[chip * NC + core, pl.ds(self.first + part * half, half)]
+        first = pl.multiple_of(self.first + self.here["core"] * half, 16)
+        return self.buffer.at[chip * NC + core, pl.ds(first, half)]
 
     def many(self, n):
         return self.buffer.at[pl.ds(0, n), pl.ds(self.first, self.rows)]
@@ -79,24 +82,27 @@
     def own(self):
         h = self.here
         mine = self.at(h["y"], h["core"])
-        self.remote(mine, self.rr.at[0], h["right"]).start()
-        self.remote(mine, self.rl.at[0], h["left"]).start()
         self.remote(mine, self.pr.at[0], h["partner"]).start()
+        self.remote(mine, self.recv.at[0], h["next"]).start()
+
+    def own2(self):
+        h = self.here
+        other = self.at(h["y"], 1 - h["core"])
+        self.remote(other, self.pr.at[0], h["partner"]).wait_recv()
+        self.remote(other, self.recv.at[1], h["next"]).start()
 
     def stage(self, d):
         h = self.here
-        for way, (rs, sign, to) in enumerate(((self.rr, -1, h["right"]), (self.rl, 1, h["left"]))):
-            chip = self.chip(sign * d)
-            got = self.at(chip, h["core"], way if d == 4 else None)
-            self.remote(got, rs.at[d - 1], to).wait_recv()
-            if d < 3:
-                self.remote(got, rs.at[d], to).start()
-            elif d == 3:
-                self.remote(self.at(chip, h["core"], way), rs.at[3], to).start()
+        chip = self.behind(d)
+        for j, core in enumerate((h["core"], 1 - h["core"])):
+            got = self.at(chip, core, d == 4)
+            self.remote(got, self.recv.at[2 * d - 2 + j], h["next"]).wait_recv()
+            if d < 4:
+                self.remote(self.at(chip, core, d == 3), self.recv.at[2 * d + j], h["next"]).start()
             self.remote(got, self.pr.at[d], h["partner"]).start()
 
     def from_partner(self, d):
-        got = self.many(2 if 0 < d < 4 else 1)
+        got = self.many(2 if d < 4 else 1)
         self.remote(got, self.pr.at[d], self.here["partner"]).wait_recv()
 
     def drain(self):
@@ -109,15 +115,15 @@
     value, gate, taps, gain, shift, wc, x, mgain, routes, rw, wg, wu, wd, sg, su, sd,
     pad, halo_out, halo_in, filt, stat, normed, slot, wslot, onehot, wide, packed, chi, clo,
     nbuf, dbuf, hbuf, cbuf, oacc, outb, rbuf,
-    load, misc, near_s, near_r, back_s, back_r, send, rr, rl, pr,
+    load, misc, near_s, near_r, back_s, back_r, send, recv, pr,
 ):
     ep, tp = lax.axis_index("ep"), lax.axis_index("tp")
     z, xx = lax.div(ep, NX), lax.rem(ep, NX)
     y, core = lax.div(tp, NC), lax.rem(tp, NC)
     here = {
         "ep": ep, "y": y, "core": core,
-        "right": lax.rem(y + 1, NY) * NC + core,
-        "left": lax.rem(y + NY - 1, NY) * NC + core,
+        "way": 1 - 2 * core,
+        "next": lax.rem(y + 1 - 2 * core + NY, NY) * NC + core,
         "partner": y * NC + (1 - core),
     }
 
@@ -152,7 +158,7 @@
         return carry
 
     def greet_ep(r, carry):
-        pl.semaphore_signal(barrier, inc=1, device_id=(lax.rem(ep + r, N_EP), tp), device_id_type=MESH)
+        pl.semaphore_signal(barrier, inc=1, device_id=(peer(N_EP - r, 1), tp), device_id_type=MESH)
         return carry
 
     lax.fori_loop(1, N_EP, greet_ep, 0)
@@ -189,6 +195,7 @@
         wide[rows, :] = dot(onehot[rows, :], mine).astype(BF16)
 
     pack(0)
+    packed[...] = dot(onehot[NEAR_ROWS:, :], normed[:, pl.ds(pl.multiple_of(tp * CH, CH), CH)]).astype(BF16)
 
     loads[3].wait()
     loads[4].wait()
@@ -215,13 +222,11 @@
     def _():
         halo.start()
 
+    lax.fori_loop(NEAR_BLOCKS, N_EP, dispatch, 0)
     dispatch_near(0)
     nbuf[core, 0:CAP, :] = wide[0:CAP, :]
-    packed[...] = dot(onehot[NEAR_ROWS:, :], normed[:, pl.ds(pl.multiple_of(tp * CH, CH), CH)]).astype(BF16)
-    lax.fori_loop(NEAR_BLOCKS, N_EP, dispatch, 0)
     for q in (1, 2):
         pack(q)
-        dispatch_near(q)
 
     loads[8].wait()
     loads[9].wait()
@@ -256,7 +261,7 @@
 
     lax.fori_loop(1, N_TP, sums, 0)
 
-    sems = (send, rr, rl, pr)
+    sems = (send, recv, pr)
     ring_d = Ring(0, dbuf, 0, FAR_ROWS, sems, here)
     ring_c = [Ring(1, cbuf, 0, CSPLIT, sems, here), Ring(2, cbuf, CSPLIT, CBROWS - CSPLIT, sems, here)]
     ring_h = [Ring(3 + g, hbuf, a, n, sems, here) for g, (a, n) in enumerate(GROUPS)]
@@ -267,7 +272,7 @@
     def take_near(q):
         first = max(CAP, q * QROWS)
         rows = pl.ds(first, (q + 1) * QROWS - first)
-        copy = remote(wide.at[rows], nbuf.at[core, rows], near_s.at[q], near_r.at[q], ep, here["right"])
+        copy = remote(wide.at[rows], nbuf.at[core, rows], near_s.at[q], near_r.at[q], ep, here["next"])
         copy.wait_recv()
         landed.append(copy)
         rows = pl.ds(q * QROWS, QROWS)
@@ -310,7 +315,7 @@
     def returned(g):
         first, end = max(CAP, GROUPS[g][0]), sum(GROUPS[g])
         rows = pl.ds(first, end - first)
-        return remote(outb.at[rows], rbuf.at[rows], back_s.at[g], back_r.at[g], ep, here["right"])
+        return remote(outb.at[rows], rbuf.at[rows], back_s.at[g], back_r.at[g], ep, here["next"])
 
     def combine(g):
         returned(g).wait_recv()
@@ -330,14 +335,15 @@
         lax.fori_loop(max(1, a // CAP), (a + n) // CAP, back, 0)
 
     def h_down(g, d):
-        ring_h[g].from_partner(d)
-        if d < 4:
-            down(g, ring_d.chip(-d), d == 0)
+        if d in (1, 2, 3):
+            down(g, ring_d.behind(d), False)
         if d > 0:
-            down(g, ring_d.chip(d), False)
+            ring_h[g].from_partner(d)
+        down(g, ring_d.behind(-d), d == 0)
 
     def conv_down(part, d):
-        ring_c[part].from_partner(d)
+        if d > 0:
+            ring_c[part].from_partner(d)
         rows = slice(part * CSPLIT, (part + 1) * CSPLIT)
         for sign in (-1, 1)[0 if 0 < d < 4 else 1 :]:
             chip = ring_d.chip(sign * d)
@@ -350,15 +356,18 @@
                 filt[rows, :] += product
 
     take_near(0)
+    dispatch_near(1)
+    dispatch_near(2)
     loads[10].wait()
     loads[11].wait()
     hidden(0)
     ring_h[0].own()
-    arrived = remote(packed, dbuf.at[tp], misc.at[0], misc.at[1], ep, here["right"])
+    arrived = remote(packed, dbuf.at[tp], misc.at[0], misc.at[1], ep, here["next"])
     arrived.wait_recv()
     ring_d.own()
+    ring_h[0].own2()
     rest = pl.ds(1, N_TP - 1)
-    summed = remote(stat.at[rest], stat.at[rest], misc.at[4], misc.at[5], ep, here["right"])
+    summed = remote(stat.at[rest], stat.at[rest], misc.at[4], misc.at[5], ep, here["next"])
     summed.wait_recv()
     total = stat[0]
     for r in range(1, N_TP):
@@ -372,6 +381,8 @@
         part = (part - turned[:, r : r + 1]) * turned[:, 4 + r : 5 + r]
         cbuf[tp, r * 128 : (r + 1) * 128, :] = silu(part * gain[...] + shift[...]).astype(BF16)
     ring_c[0].own()
+    ring_d.own2()
+    ring_c[0].own2()
     ring_h[0].stage(1)
     ring_d.stage(1)
     ring_c[0].stage(1)
@@ -383,13 +394,14 @@
     dispatch_near(3)
     pack(4)
     dispatch_near(4)
+    ring_h[0].stage(2)
     hidden(1)
     hidden(2)
     ring_h[3].own()
-    ring_h[0].stage(2)
     ring_d.stage(2)
     ring_c[0].stage(2)
     h_down(0, 1)
+    ring_h[3].own2()
     ring_h[0].stage(3)
     ring_d.stage(3)
     ring_c[0].stage(3)
@@ -400,12 +412,13 @@
     ring_h[0].stage(4)
     ring_c[0].stage(4)
     ring_h[3].stage(2)
-    for d in range(5):
+    for d in range(1, 5):
         ring_d.from_partner(d)
     hidden(5)
     hidden(6)
     hidden(7)
     ring_h[1].own()
+    ring_h[1].own2()
     h_down(0, 3)
     h_down(0, 4)
     give_back(0)
@@ -415,6 +428,7 @@
     hidden(4)
     ring_h[2].own()
     ring_h[3].stage(3)
+    ring_h[2].own2()
     h_down(3, 1)
     h_down(3, 2)
     ring_h[1].stage(1)
@@ -430,6 +444,7 @@
     ring_c[1].own()
     h_down(1, 1)
     h_down(2, 1)
+    ring_c[1].own2()
     loads[12].wait()
     for d in range(5):
         conv_down(0, d)
@@ -450,13 +465,13 @@
         hot = onehot[r * CAP : (r + 1) * CAP, :].astype(F32)
         chi[r * CAP : (r + 1) * CAP, :] = (hot * high).astype(BF16)
         clo[r * CAP : (r + 1) * CAP, :] = (hot * (w - high)).astype(BF16)
+    h_down(1, 3)
+    h_down(2, 3)
     ring_h[1].stage(4)
     ring_h[2].stage(4)
-    ring_c[1].stage(2)
-    h_down(1, 3)
     h_down(1, 4)
     give_back(1)
-    h_down(2, 3)
+    ring_c[1].stage(2)
     h_down(2, 4)
     give_back(2)
     ring_c[1].stage(3)
@@ -532,8 +547,7 @@
             dma((len(GROUPS),)),
             dma((len(GROUPS),)),
             dma((rings,)),
-            dma((rings, 4)),
-            dma((rings, 4)),
+            dma((rings, 8)),
             dma((rings, 5)),
         ],
         compiler_params=pltpu.CompilerParams(

time: 96.9 us -> 94.3 us (0.973)
  Pallas kernels: 94.1 us -> 92.3 us
    pallas_call x1, Pallas kernels: 94.1 us -> 92.3 us  [body(): pl.pallas_call(kernel, out_shape=outs, in_specs=[pl.BlockSpec(memory_spac...]
where the time goes in v4:
time: 94.3 us; the launch traced here: 94.2 us
  Pallas kernels  92.3 us (98%)
  local copies, waits for them, and re-layouts  1.27 us (1%)
    pallas_call x1, Pallas kernels, body(): pl.pallas_call(kernel, out_shape=outs, in_specs=[pl.BlockSpec(memory_spac...  92.3 us

profile of v4, /device:TPU:1, one launch (start us, length us, event | category | flops | bytes accessed | tf_op | source)
XLA Modules:
  0.0 94.2 jit_solution(16157465671533661479)
XLA Ops:
  0.6 92.3 %shard_map.167 = (bf16[512,128]{1,0:T(8,128)(2,1)S(1)}, bf16[128,128]{1,0:T(8,128)(2,1)S(1)}) custom-call(bf16[512,128]{1,0:T(8,128)(2,1)} %value_h.1, bf16[512,128]{1,0:T(8,128)(2,1)} %gate_h.1, f32[31,128]{1,0:T(8,128)} %taps_h.1, f32[1,128]{1,0:T(1,128)} %bitcast.18, f32[1,128]{1,0:T(1,128)} %bitcast.19, bf16[2048,128]{1,0:T(8,128)(2,1)} %wc_h.1, ...), custom_call_target="tpu_custom_call" | custom-call | flops 5000000000 | bytes 8000000 | tf_op jit(solution)/shard_map/pallas_call | solution.py:516
  92.9 0.7 copy.20
  93.6 0.6 copy.21

commit v5 on v4

--- a/solution.py
+++ b/solution.py
@@ -32,7 +32,7 @@
 WIDE = D // NC
 GROUPS = ((0, 128), (640, 384), (384, 256), (128, 256))
 CBROWS = ROWS_A + SH
-CSPLIT = ROWS_A // 2
+CSPLIT = 128
 
 
 def dot(a, b, dims=(((1,), (0,)), ((), ())), precision=None):
@@ -127,11 +127,18 @@
         "partner": y * NC + (1 - core),
     }
 
+    z_at = [lax.rem(z + d, NZ) * NX for d in range(NZ)]
+    x_at = [lax.rem(xx + d, NX) for d in range(NX)]
+    y_at = [lax.rem(y + d, NY) * NC for d in range(NY)]
+    core_at = [core, 1 - core]
+
     def peer(rho, sign):
-        q, dx = lax.div(rho, NX), lax.rem(rho, NX)
-        odd = lax.rem(q, 2)
-        dz = odd * lax.div(q + 1, 2) + (1 - odd) * lax.rem(NZ - lax.div(q, 2), NZ)
-        return lax.rem(z + sign * dz + NZ, NZ) * NX + lax.rem(xx + sign * dx + NX, NX)
+        q, dx = divmod(rho, NX)
+        dz = (q + 1) // 2 if q % 2 else (NZ - q // 2) % NZ
+        return z_at[sign * dz % NZ] + x_at[sign * dx % NX]
+
+    def tp_peer(r):
+        return y_at[r // NC] + core_at[r % NC]
 
     def remote(src, dst, send, recv, to_ep, to_tp):
         return pltpu.make_async_remote_copy(
@@ -148,31 +155,17 @@
             )
         )
     ]
-    for copy in loads[:5]:
-        copy.start()
+    for i in (2, 3, 4, 1, 0):
+        loads[i].start()
 
     barrier = pltpu.get_barrier_semaphore()
 
-    def greet_tp(r, carry):
-        pl.semaphore_signal(barrier, inc=1, device_id=(ep, lax.rem(tp + r, N_TP)), device_id_type=MESH)
-        return carry
-
-    def greet_ep(r, carry):
-        pl.semaphore_signal(barrier, inc=1, device_id=(peer(N_EP - r, 1), tp), device_id_type=MESH)
-        return carry
-
-    lax.fori_loop(1, N_EP, greet_ep, 0)
-    lax.fori_loop(1, N_TP, greet_tp, 0)
-
-    for copy in loads[5:]:
-        copy.start()
-
-    for i in range(3):
-        loads[i].wait()
-    for r in range(0, TOK, 32):
-        rows = x[r : r + 32, :].astype(F32)
-        mean = jnp.mean(rows * rows, axis=1, keepdims=True)
-        normed[r : r + 32, :] = (rows * lax.rsqrt(mean + 1e-06) * mgain[...]).astype(BF16)
+    for r in range(N_EP - 1, 0, -1):
+        pl.semaphore_signal(barrier, inc=1, device_id=(peer(r, 1), tp), device_id_type=MESH)
+    for r in range(N_TP - 1, 0, -1):
+        pl.semaphore_signal(barrier, inc=1, device_id=(ep, tp_peer(r)), device_id_type=MESH)
+
+    loads[2].wait()
     rho = lax.broadcasted_iota(jnp.int32, (N_EP, TOK), 0)
     q, dx = rho >> 2, rho & 3
     dz = jnp.where((q & 1) == 1, (q + 1) >> 1, (NZ - (q >> 1)) & 7)
@@ -189,13 +182,6 @@
     for r in range(N_EP):
         onehot[r * CAP : (r + 1) * CAP, :] = jnp.where(slot[r : r + 1, :] == place, 1.0, 0.0).astype(BF16)
 
-    def pack(q):
-        rows = slice(q * QROWS, (q + 1) * QROWS)
-        mine = normed[:, pl.ds(pl.multiple_of(core * WIDE, WIDE), WIDE)]
-        wide[rows, :] = dot(onehot[rows, :], mine).astype(BF16)
-
-    pack(0)
-    packed[...] = dot(onehot[NEAR_ROWS:, :], normed[:, pl.ds(pl.multiple_of(tp * CH, CH), CH)]).astype(BF16)
 
     loads[3].wait()
     loads[4].wait()
@@ -203,27 +189,42 @@
     pad[HALO:, :] = glu.astype(F32)
     halo_out[...] = glu[ROWS_A - HALO :, :]
     halo = remote(halo_out, halo_in, misc.at[2], misc.at[3], lax.rem(ep + 1, N_EP), tp)
+
+    loads[1].wait()
+    loads[0].wait()
+    for r in range(0, TOK, 32):
+        rows = x[r : r + 32, :].astype(F32)
+        mean = jnp.mean(rows * rows, axis=1, keepdims=True)
+        normed[r : r + 32, :] = (rows * lax.rsqrt(mean + 1e-06) * mgain[...]).astype(BF16)
+
+    def pack(q):
+        rows = slice(q * QROWS, (q + 1) * QROWS)
+        mine = normed[:, pl.ds(pl.multiple_of(core * WIDE, WIDE), WIDE)]
+        wide[rows, :] = dot(onehot[rows, :], mine).astype(BF16)
+
+    pack(0)
+    packed[...] = dot(onehot[NEAR_ROWS:, :], normed[:, pl.ds(pl.multiple_of(tp * CH, CH), CH)]).astype(BF16)
+
     pl.semaphore_wait(barrier, N_TP - 1 + N_EP - 1)
 
-    def dispatch(r, carry):
-        rows = pl.ds((r - NEAR_BLOCKS) * CAP, CAP)
-        remote(packed.at[rows], dbuf.at[tp, rows], misc.at[0], misc.at[1], peer(r, 1), tp).start()
-        return carry
+    def dispatch_far():
+        for r in range(N_EP - 1, NEAR_BLOCKS - 1, -1):
+            rows = pl.ds((r - NEAR_BLOCKS) * CAP, CAP)
+            remote(packed.at[rows], dbuf.at[tp, rows], misc.at[0], misc.at[1], peer(r, 1), tp).start()
 
     def dispatch_near(q):
-        def step(r, carry):
+        for r in range(max(1, q * NX), (q + 1) * NX):
             rows = pl.ds(r * CAP, CAP)
-            remote(wide.at[rows], nbuf.at[core, rows], near_s.at[q], near_r.at[q], peer(r, 1), tp).start()
-            return carry
-
-        lax.fori_loop(max(1, q * NX), (q + 1) * NX, step, 0)
+            remote(wide.at[rows], nbuf.at[core, rows], near_s.at[0], near_r.at[q], peer(r, 1), tp).start()
 
     @pl.when(ep < N_EP - 1)
     def _():
         halo.start()
 
-    lax.fori_loop(NEAR_BLOCKS, N_EP, dispatch, 0)
+    dispatch_far()
     dispatch_near(0)
+    for copy in loads[5:]:
+        copy.start()
     nbuf[core, 0:CAP, :] = wide[0:CAP, :]
     for q in (1, 2):
         pack(q)
@@ -255,37 +256,27 @@
         stat[0, r : r + 1, :] = dot(ones, part, NT, lax.Precision.HIGHEST)[0:1, :]
         stat[0, 4 + r : 5 + r, :] = dot(ones, part * part, NT, lax.Precision.HIGHEST)[0:1, :]
 
-    def sums(r, carry):
-        remote(stat.at[0], stat.at[r], misc.at[4], misc.at[5], ep, lax.rem(tp + r, N_TP)).start()
-        return carry
-
-    lax.fori_loop(1, N_TP, sums, 0)
+    for r in range(N_TP - 1, 0, -1):
+        remote(stat.at[0], stat.at[r], misc.at[4], misc.at[5], ep, tp_peer(r)).start()
 
     sems = (send, recv, pr)
     ring_d = Ring(0, dbuf, 0, FAR_ROWS, sems, here)
     ring_c = [Ring(1, cbuf, 0, CSPLIT, sems, here), Ring(2, cbuf, CSPLIT, CBROWS - CSPLIT, sems, here)]
     ring_h = [Ring(3 + g, hbuf, a, n, sems, here) for g, (a, n) in enumerate(GROUPS)]
 
-    passed = []
-    landed = []
-
     def take_near(q):
         first = max(CAP, q * QROWS)
         rows = pl.ds(first, (q + 1) * QROWS - first)
-        copy = remote(wide.at[rows], nbuf.at[core, rows], near_s.at[q], near_r.at[q], ep, here["next"])
-        copy.wait_recv()
-        landed.append(copy)
+        remote(wide.at[rows], nbuf.at[core, rows], near_s.at[0], near_r.at[q], ep, here["next"]).wait_recv()
         rows = pl.ds(q * QROWS, QROWS)
-        copy = remote(
-            nbuf.at[core, rows], nbuf.at[core, rows], near_s.at[NEAR + q], near_r.at[NEAR + q], ep, here["partner"]
-        )
-        copy.start()
-        passed.append(copy)
+        remote(
+            nbuf.at[core, rows], nbuf.at[core, rows], near_s.at[1], near_r.at[NEAR + q], ep, here["partner"]
+        ).start()
 
     def near_from_partner(q):
         rows = pl.ds(q * QROWS, QROWS)
         remote(
-            nbuf.at[1 - core, rows], nbuf.at[1 - core, rows], near_s.at[NEAR + q], near_r.at[NEAR + q],
+            nbuf.at[1 - core, rows], nbuf.at[1 - core, rows], near_s.at[1], near_r.at[NEAR + q],
             ep, here["partner"],
         ).wait_recv()
 
@@ -315,7 +306,7 @@
     def returned(g):
         first, end = max(CAP, GROUPS[g][0]), sum(GROUPS[g])
         rows = pl.ds(first, end - first)
-        return remote(outb.at[rows], rbuf.at[rows], back_s.at[g], back_r.at[g], ep, here["next"])
+        return remote(outb.at[rows], rbuf.at[rows], back_s.at[0], back_r.at[g], ep, here["next"])
 
     def combine(g):
         returned(g).wait_recv()
@@ -327,12 +318,9 @@
         a, n = GROUPS[g]
         outb[a : a + n, :] = oacc[a : a + n, :].astype(BF16)
 
-        def back(r, carry):
+        for r in range(max(1, a // CAP), (a + n) // CAP):
             rows = pl.ds(r * CAP, CAP)
-            remote(outb.at[rows], rbuf.at[rows], back_s.at[g], back_r.at[g], peer(r, -1), tp).start()
-            return carry
-
-        lax.fori_loop(max(1, a // CAP), (a + n) // CAP, back, 0)
+            remote(outb.at[rows], rbuf.at[rows], back_s.at[0], back_r.at[g], peer(r, -1), tp).start()
 
     def h_down(g, d):
         if d in (1, 2, 3):
@@ -344,7 +332,7 @@
     def conv_down(part, d):
         if d > 0:
             ring_c[part].from_partner(d)
-        rows = slice(part * CSPLIT, (part + 1) * CSPLIT)
+        rows = slice(part * CSPLIT, (CSPLIT, ROWS_A)[part])
         for sign in (-1, 1)[0 if 0 < d < 4 else 1 :]:
             chip = ring_d.chip(sign * d)
             depth = pl.ds(pl.multiple_of(chip * NC * CH, NC * CH), NC * CH)
@@ -395,11 +383,11 @@
     pack(4)
     dispatch_near(4)
     ring_h[0].stage(2)
+    ring_d.stage(2)
+    ring_c[0].stage(2)
     hidden(1)
     hidden(2)
     ring_h[3].own()
-    ring_d.stage(2)
-    ring_c[0].stage(2)
     h_down(0, 1)
     ring_h[3].own2()
     ring_h[0].stage(3)
@@ -493,7 +481,12 @@
     def _():
         halo.wait_send()
 
-    for copy in (arrived, summed, *[returned(g) for g in range(len(GROUPS))], *landed, *passed):
+    rest = pl.ds(CAP, NEAR_ROWS - CAP)
+    landed = remote(wide.at[rest], nbuf.at[core, rest], near_s.at[0], near_r.at[0], ep, here["next"])
+    passed = remote(nbuf.at[core], nbuf.at[core], near_s.at[1], near_r.at[NEAR], ep, here["partner"])
+    rest = pl.ds(CAP, SLOTS - CAP)
+    returning = remote(outb.at[rest], rbuf.at[rest], back_s.at[0], back_r.at[0], ep, here["next"])
+    for copy in (arrived, summed, landed, passed, returning):
         copy.wait_send()
     for ring in (ring_d, *ring_c, *ring_h):
         ring.drain()
@@ -542,9 +535,9 @@
             vmem((SLOTS, CH), BF16),
             dma((16,)),
             dma((6,)),
+            dma((2,)),
             dma((2 * NEAR,)),
-            dma((2 * NEAR,)),
-            dma((len(GROUPS),)),
+            dma((1,)),
             dma((len(GROUPS),)),
             dma((rings,)),
             dma((rings, 8)),

time: 94.3 us -> 93 us (0.986)
  Pallas kernels: 92.3 us -> 90.7 us
    pallas_call x1, Pallas kernels: 92.3 us -> 90.7 us  [body(): pl.pallas_call(kernel, out_shape=outs, in_specs=[pl.BlockSpec(memory_spac...]
where the time goes in v5:
time: 93 us; the launch traced here: 92.7 us
  Pallas kernels  90.7 us (98%)
  local copies, waits for them, and re-layouts  1.27 us (1%)
    pallas_call x1, Pallas kernels, body(): pl.pallas_call(kernel, out_shape=outs, in_specs=[pl.BlockSpec(memory_spac...  90.7 us

profile of v5, /device:TPU:1, one launch (start us, length us, event | category | flops | bytes accessed | tf_op | source)
XLA Modules:
  0.0 92.7 jit_solution(10744283035477005303)
XLA Ops:
  0.6 90.7 %shard_map.167 = (bf16[512,128]{1,0:T(8,128)(2,1)S(1)}, bf16[128,128]{1,0:T(8,128)(2,1)S(1)}) custom-call(bf16[512,128]{1,0:T(8,128)(2,1)} %value_h.1, bf16[512,128]{1,0:T(8,128)(2,1)} %gate_h.1, f32[31,128]{1,0:T(8,128)} %taps_h.1, f32[1,128]{1,0:T(1,128)} %bitcast.18, f32[1,128]{1,0:T(1,128)} %bitcast.19, bf16[2048,128]{1,0:T(8,128)(2,1)} %wc_h.1, ...), custom_call_target="tpu_custom_call" | custom-call | flops 5000000000 | bytes 8000000 | tf_op jit(solution)/shard_map/pallas_call | solution.py:509
  91.4 0.7 copy.20
  92.0 0.6 copy.21

commit v6 on v5

--- a/solution.py
+++ b/solution.py
@@ -113,7 +113,7 @@
     value_h, gate_h, taps_h, gain_h, shift_h, wc_h, x_h, mgain_h, routes_h, rw_h, wg_h, wu_h, wd_h, sg_h, su_h, sd_h,
     conv_o, moe_o,
     value, gate, taps, gain, shift, wc, x, mgain, routes, rw, wg, wu, wd, sg, su, sd,
-    pad, halo_out, halo_in, filt, stat, normed, slot, wslot, onehot, wide, packed, chi, clo,
+    pad, halo_out, halo_in, filt, stat, normed, slot, wslot, onehot, wide, packed, chi, clo, high_t, low_t,
     nbuf, dbuf, hbuf, cbuf, oacc, outb, rbuf,
     load, misc, near_s, near_r, back_s, back_r, send, recv, pr,
 ):
@@ -312,13 +312,13 @@
         returned(g).wait_recv()
         a, n = GROUPS[g]
         rows = slice(a, a + n)
-        return dot(chi[rows, :], rbuf[rows, :], TN) + dot(clo[rows, :], rbuf[rows, :], TN)
+        return dot(high_t[:, rows], rbuf[rows, :]) + dot(low_t[:, rows], rbuf[rows, :])
 
     def give_back(g):
         a, n = GROUPS[g]
         outb[a : a + n, :] = oacc[a : a + n, :].astype(BF16)
 
-        for r in range(max(1, a // CAP), (a + n) // CAP):
+        for r in range((a + n) // CAP - 1, max(1, a // CAP) - 1, -1):
             rows = pl.ds(r * CAP, CAP)
             remote(outb.at[rows], rbuf.at[rows], back_s.at[0], back_r.at[g], peer(r, -1), tp).start()
 
@@ -453,6 +453,8 @@
         hot = onehot[r * CAP : (r + 1) * CAP, :].astype(F32)
         chi[r * CAP : (r + 1) * CAP, :] = (hot * high).astype(BF16)
         clo[r * CAP : (r + 1) * CAP, :] = (hot * (w - high)).astype(BF16)
+    high_t[...] = chi[...].T
+    low_t[...] = clo[...].T
     h_down(1, 3)
     h_down(2, 3)
     ring_h[1].stage(4)
@@ -526,6 +528,8 @@
             vmem((FAR_ROWS, CH), BF16),
             vmem((SLOTS, TOK), BF16),
             vmem((SLOTS, TOK), BF16),
+            vmem((TOK, SLOTS), BF16),
+            vmem((TOK, SLOTS), BF16),
             vmem((NC, NEAR_ROWS, WIDE), BF16),
             vmem((N_TP, FAR_ROWS, CH), BF16),
             vmem((N_TP, SLOTS, HID), BF16),

time: 93 us -> 92.7 us (level)
  no operation moved by 1% of the time
where the time goes in v6:
time: 92.7 us; the launch traced here: 92.6 us
  Pallas kernels  90.7 us (98%)
  local copies, waits for them, and re-layouts  1.27 us (1%)
    pallas_call x1, Pallas kernels, body(): pl.pallas_call(kernel, out_shape=outs, in_specs=[pl.BlockSpec(memory_spac...  90.7 us

profile of v6, /device:TPU:1, one launch (start us, length us, event | category | flops | bytes accessed | tf_op | source)
XLA Modules:
  0.0 92.6 jit_solution(3344461289587649850)
XLA Ops:
  0.6 90.7 %shard_map.167 = (bf16[512,128]{1,0:T(8,128)(2,1)S(1)}, bf16[128,128]{1,0:T(8,128)(2,1)S(1)}) custom-call(bf16[512,128]{1,0:T(8,128)(2,1)} %value_h.1, bf16[512,128]{1,0:T(8,128)(2,1)} %gate_h.1, f32[31,128]{1,0:T(8,128)} %taps_h.1, f32[1,128]{1,0:T(1,128)} %bitcast.18, f32[1,128]{1,0:T(1,128)} %bitcast.19, bf16[2048,128]{1,0:T(8,128)(2,1)} %wc_h.1, ...), custom_call_target="tpu_custom_call" | custom-call | flops 5000000000 | bytes 8000000 | tf_op jit(solution)/shard_map/pallas_call | solution.py:511
  91.3 0.7 copy.20
  92.0 0.6 copy.21
